TPU v7x, 256 devices: a whole 4x4x8 slice. The times are simulated.
256 devices in a mesh: sp: 128 (over z, y, x), tp: 2 (over core).
Axes of the slice: x: 4, y: 4, z: 8, core: 2. Of those that a mesh axis runs over, the one named last changes fastest.
Arguments:
- queries: bfloat16 [3, 32768, 2048], P(None, 'sp', 'tp'), may hold values from -6 to 6
- keys: bfloat16 [3, 32768, 2048], P(None, 'sp', 'tp'), may hold values from -6 to 6
- values: bfloat16 [3, 32768, 2048], P(None, 'sp', 'tp'), may hold values from -6 to 6
- w_out: bfloat16 [2048, 2048], P(None, 'tp'), may hold values from -1 to 1
Outputs:
- mixed: bfloat16 [32768, 2048], P('sp', 'tp')
All inputs are finite; a program needn't handle non-finite values.
Results may differ from a plain program's by a relative error of at most 0.01.
Values may be sent and summed in bfloat16 or wider, within the bound.
No kernel may reach another device: no remote copies, remote signals or barrier semaphores. Data moves between devices by JAX's collectives and lax.ppermute only.
A program may use at most 128 MiB of HBM per device.

v0:
```python
import functools

import jax
import jax.numpy as jnp
from jax import lax
from jax.experimental import pallas as pl
from jax.experimental.pallas import tpu as pltpu
from jax.sharding import PartitionSpec as P


HEAD = 128
WINDOW = 128
ROPE_BASE = 10000.0
MASKED = -1e30
SCALE = HEAD ** (-0.5)

TOKENS = 256
LOCAL = 8
PLANE = 16
HALF = TOKENS // 2
ROW = 4
ROW_HEADS = LOCAL // ROW
RETURN_ROWS = HALF + 16
ROW_RETURN = TOKENS + 16


f32 = jnp.float32
bf16 = jnp.bfloat16


def iota(shape, dim):
    return lax.broadcasted_iota(jnp.int32, shape, dim)


def turned(x, cosine, sine):
    x = x.astype(f32)
    return x * cosine + pltpu.roll(x, HEAD // 2, 1) * sine


def full_tables(cos_ref, sin_ref):
    cosine, sine = cos_ref[...], sin_ref[...]
    return jnp.concatenate([cosine, cosine], axis=1), jnp.concatenate([-sine, sine], axis=1)


def fetched(sources, target, sem):
    copies = [pltpu.make_async_copy(ref, target.at[a], sem.at[a]) for a, ref in enumerate(sources)]
    for copy in copies:
        copy.start()
    return copies


def turned_as(kind, x, cosine, sine):
    if kind == "v":
        return x.astype(f32)
    return turned(x, cosine, sine) * (SCALE if kind == "q" else 1.0)


def plane_pieces_kernel(cos_ref, sin_ref, k_ref, v_ref, q_ref, out_ref, in_ref, sort_ref, piece_ref, sem, out_sem):
    copies = fetched([ref.at[2] for ref in (k_ref, v_ref, q_ref)], in_ref, sem)
    cosine, sine = full_tables(cos_ref, sin_ref)
    stores = []
    for a, kind in enumerate("kvq"):
        copies[a].wait()
        for h in range(LOCAL):
            sort_ref[h] = turned_as(kind, in_ref[a, :, h * HEAD : (h + 1) * HEAD], cosine, sine)
            for p in range(2):
                rows = [sort_ref[h, pl.ds(p + 2 * r, 16, stride=16), :] for r in range(8)]
                piece_ref[2 * h + p, a] = jnp.concatenate(rows, axis=0).astype(bf16)
        stores.append(pltpu.make_async_copy(piece_ref.at[:, a], out_ref.at[:, a], out_sem.at[a]))
        stores[-1].start()
    for store in stores:
        store.wait()


def plane_pieces(keys, values, queries, cosine, sine):
    vmem, hbm = pl.BlockSpec(memory_space=pltpu.VMEM), pl.BlockSpec(memory_space=pltpu.HBM)
    shape = (PLANE, 3, HALF, HEAD)
    return pl.pallas_call(
        plane_pieces_kernel,
        in_specs=[vmem, vmem, hbm, hbm, hbm],
        out_specs=hbm,
        scratch_shapes=[
            pltpu.VMEM((3, TOKENS, LOCAL * HEAD), bf16),
            pltpu.VMEM((LOCAL, TOKENS, HEAD), f32),
            pltpu.VMEM(shape, bf16),
            pltpu.SemaphoreType.DMA((3,)),
            pltpu.SemaphoreType.DMA((3,)),
        ],
        out_shape=jax.ShapeDtypeStruct(shape, bf16),
        cost_estimate=pl.CostEstimate(flops=2**30, bytes_accessed=3 * 2**20, transcendentals=0),
        name="plane_pieces",
    )(cosine, sine, keys, values, queries)


def row_pieces_kernel(x_ref, cos_ref, sin_ref, k_ref, v_ref, q_ref, *refs):
    outs = refs[:ROW]
    in_ref, sort_ref, piece_ref, sem, out_sem = refs[ROW:]
    copies = fetched([ref.at[1] for ref in (k_ref, v_ref, q_ref)], in_ref, sem)
    cosine, sine = full_tables(cos_ref, sin_ref)
    stores = []

    def store(source, target, index):
        stores.append(pltpu.make_async_copy(source, target, out_sem.at[index]))
        stores[-1].start()

    for a, kind in enumerate("kvq"):
        copies[a].wait()
        for steps in range(ROW):
            chip = lax.rem(x_ref[0] + steps, ROW)
            for h in range(ROW_HEADS):
                lanes = pl.ds(pl.multiple_of((chip * ROW_HEADS + h) * HEAD, HEAD), HEAD)
                slot = steps * ROW_HEADS + h
                sort_ref[slot] = turned_as(kind, in_ref[a, :, lanes], cosine, sine)
                rows = [sort_ref[slot, pl.ds(r, 64, stride=4), :] for r in range(4)]
                piece_ref[steps, a, h] = jnp.concatenate(rows, axis=0).astype(bf16)
            store(piece_ref.at[steps, a], outs[steps].at[a], a * ROW + steps)
    for copy in stores:
        copy.wait()


def row_pieces(x, keys, values, queries, cosine, sine):
    vmem, hbm = pl.BlockSpec(memory_space=pltpu.VMEM), pl.BlockSpec(memory_space=pltpu.HBM)
    shape = (ROW_HEADS, TOKENS, HEAD)
    return pl.pallas_call(
        row_pieces_kernel,
        in_specs=[pl.BlockSpec(memory_space=pltpu.SMEM), vmem, vmem, hbm, hbm, hbm],
        out_specs=[hbm] * ROW,
        scratch_shapes=[
            pltpu.VMEM((3, TOKENS, LOCAL * HEAD), bf16),
            pltpu.VMEM((LOCAL, TOKENS, HEAD), f32),
            pltpu.VMEM((ROW, 3, *shape), bf16),
            pltpu.SemaphoreType.DMA((3,)),
            pltpu.SemaphoreType.DMA((3 * ROW,)),
        ],
        out_shape=[jax.ShapeDtypeStruct((3, *shape), bf16)] * ROW,
        cost_estimate=pl.CostEstimate(flops=2**30, bytes_accessed=3 * 2**20, transcendentals=0),
        name="row_pieces",
    )(x, cosine, sine, keys, values, queries)


def dot_t(a, b):
    return lax.dot_general(a, b, (((1,), (1,)), ((), ())), preferred_element_type=f32)


def attend(q, k_prev, k_cur, v_prev, v_cur, prev_bias):
    row = iota((WINDOW, 2 * WINDOW), 0)
    col = iota((WINDOW, 2 * WINDOW), 1)
    scores = dot_t(q, jnp.concatenate([k_prev, k_cur], axis=0))
    scores = jnp.where((col >= row) & (col <= row + WINDOW), scores, MASKED)
    if prev_bias is not None:
        scores = jnp.minimum(scores, jnp.where(iota((1, 2 * WINDOW), 1) < WINDOW, prev_bias, -MASKED))
    row_max = jnp.max(scores, axis=1, keepdims=True)
    probs = jnp.exp(scores - row_max)
    row_sum = jnp.sum(probs, axis=1, keepdims=True)
    total = jnp.dot(probs.astype(bf16), jnp.concatenate([v_prev, v_cur], axis=0), preferred_element_type=f32)
    return total / row_sum, row_max + jnp.log(row_sum)


def wide(column):
    return jnp.broadcast_to(column, (column.shape[0], HEAD))


def column_to_rows(column):
    eye = iota((HALF, HEAD), 0) == iota((HALF, HEAD), 1)
    ones = jnp.ones((16, HALF), bf16)
    column = wide(column)
    high = column.astype(bf16)
    low = (column - high.astype(f32)).astype(bf16)
    zero = jnp.zeros_like(high)
    high = jnp.dot(ones, jnp.where(eye, high, zero), preferred_element_type=f32)
    low = jnp.dot(ones, jnp.where(eye, low, zero), preferred_element_type=f32)
    return jnp.where(iota((16, HEAD), 0) % 2 == 0, high, low)


def rows_to_column(high, low):
    eye = iota((HALF, HEAD), 0) == iota((HALF, HEAD), 1)
    ones = jnp.ones((HEAD, HEAD), bf16)
    zero = jnp.zeros((HALF, HEAD), bf16)
    return sum(
        jnp.dot(jnp.where(eye, jnp.broadcast_to(part, (HALF, HEAD)), zero), ones, preferred_element_type=f32)
        for part in (high, low)
    )


def plane_kernel(z_ref, in_ref, halo_ref, out_ref, logs_ref):
    bias = jnp.where(z_ref[0] == 0, MASKED, -MASKED)
    for r in range(8):
        rows = slice(r * 16, (r + 1) * 16)
        ks = [jnp.concatenate([halo_ref[i, 0, rows, :] for i in range(8)], axis=0)]
        vs = [jnp.concatenate([halo_ref[i, 1, rows, :] for i in range(8)], axis=0)]
        for b in range(2):
            chips = range(8 * b, 8 * b + 8)
            ks.append(jnp.concatenate([in_ref[s, 0, rows, :] for s in chips], axis=0))
            vs.append(jnp.concatenate([in_ref[s, 1, rows, :] for s in chips], axis=0))
            q = jnp.concatenate([in_ref[s, 2, rows, :] for s in chips], axis=0)
            result, logs = attend(q, ks[b], ks[b + 1], vs[b], vs[b + 1], bias if b == 0 else None)
            for i, s in enumerate(chips):
                out_ref[s, rows, :] = result[i * 16 : (i + 1) * 16].astype(bf16)
                logs_ref[s, rows, :] = logs[i * 16 : (i + 1) * 16]
    for s in range(PLANE):
        out_ref[s, HALF:, :] = column_to_rows(logs_ref[s]).astype(bf16)


def plane_attention(z, held, halo):
    vmem = pl.BlockSpec(memory_space=pltpu.VMEM)
    return pl.pallas_call(
        plane_kernel,
        in_specs=[pl.BlockSpec(memory_space=pltpu.SMEM), vmem, vmem],
        out_specs=vmem,
        out_shape=jax.ShapeDtypeStruct((PLANE, RETURN_ROWS, HEAD), bf16),
        scratch_shapes=[pltpu.VMEM((PLANE, HALF, 1), f32)],
        compiler_params=pltpu.CompilerParams(vmem_limit_bytes=8 * 2**20),
        cost_estimate=pl.CostEstimate(flops=2**31, bytes_accessed=3 * 2**20, transcendentals=2**19),
        name="plane_attention",
    )(z, held, halo)


def pick_kernel(x_ref, own_ref, one_ref, two_ref, three_ref, out_ref):
    x = x_ref[0]
    for steps, ref in enumerate((own_ref, one_ref, two_ref, three_ref)):
        chip = lax.rem(x + ROW - steps, ROW)

        @pl.when(chip >= ROW // 2)
        def _(ref=ref, chip=chip):
            out_ref[chip - ROW // 2] = ref[:2]


def pick_last(x, pieces):
    vmem = pl.BlockSpec(memory_space=pltpu.VMEM)
    return pl.pallas_call(
        pick_kernel,
        in_specs=[pl.BlockSpec(memory_space=pltpu.SMEM)] + [vmem] * ROW,
        out_specs=vmem,
        out_shape=jax.ShapeDtypeStruct((2, 2, ROW_HEADS, TOKENS, HEAD), bf16),
        compiler_params=pltpu.CompilerParams(vmem_limit_bytes=4 * 2**20),
        cost_estimate=pl.CostEstimate(flops=2**20, bytes_accessed=2**21, transcendentals=0),
        name="pick_last",
    )(x, *pieces)


def row_kernel(x_ref, *refs):
    ins, halo_ref, outs = refs[:ROW], refs[ROW], refs[ROW + 1 : 2 * ROW + 1]
    in_ref, res_ref, logs_ref = refs[2 * ROW + 1 :]
    x = x_ref[0]
    bias = jnp.where(x_ref[1] == 0, MASKED, -MASKED)
    for steps in range(ROW):
        in_ref[lax.rem(x + ROW - steps, ROW)] = ins[steps][...]
    for h in range(ROW_HEADS):
        for r in range(4):
            rows = slice(r * 64, (r + 1) * 64)
            ks = [jnp.concatenate([halo_ref[i, 0, h, rows, :] for i in range(2)], axis=0)]
            vs = [jnp.concatenate([halo_ref[i, 1, h, rows, :] for i in range(2)], axis=0)]
            for b in range(2):
                chips = (2 * b, 2 * b + 1)
                ks.append(jnp.concatenate([in_ref[s, 0, h, rows, :] for s in chips], axis=0))
                vs.append(jnp.concatenate([in_ref[s, 1, h, rows, :] for s in chips], axis=0))
                q = jnp.concatenate([in_ref[s, 2, h, rows, :] for s in chips], axis=0)
                result, logs = attend(q, ks[b], ks[b + 1], vs[b], vs[b + 1], bias if b == 0 else None)
                for i, s in enumerate(chips):
                    res_ref[s, h, rows, :] = result[i * 64 : (i + 1) * 64].astype(bf16)
                    logs_ref[s, h, rows, :] = logs[i * 64 : (i + 1) * 64]
    sub = iota((16, HEAD), 0)
    for s in range(ROW):
        for h in range(ROW_HEADS):
            tiles = [column_to_rows(logs_ref[s, h, half * HALF : (half + 1) * HALF, :]) for half in range(2)]
            res_ref[s, h, TOKENS:, :] = jnp.where(sub < 2, tiles[0], tiles[1]).astype(bf16)
    for steps, out in enumerate(outs):
        out[...] = res_ref[lax.rem(x + steps, ROW)]


def row_attention(place, pieces, halo):
    shape = (ROW_HEADS, ROW_RETURN, HEAD)
    vmem = pl.BlockSpec(memory_space=pltpu.VMEM)
    return pl.pallas_call(
        row_kernel,
        in_specs=[pl.BlockSpec(memory_space=pltpu.SMEM)] + [vmem] * (ROW + 1),
        out_specs=[vmem] * ROW,
        out_shape=[jax.ShapeDtypeStruct(shape, bf16)] * ROW,
        scratch_shapes=[
            pltpu.VMEM((ROW, 3, ROW_HEADS, TOKENS, HEAD), bf16),
            pltpu.VMEM((ROW, *shape), bf16),
            pltpu.VMEM((ROW, ROW_HEADS, TOKENS, 1), f32),
        ],
        compiler_params=pltpu.CompilerParams(vmem_limit_bytes=12 * 2**20),
        cost_estimate=pl.CostEstimate(flops=2**31, bytes_accessed=3 * 2**20, transcendentals=2**19),
        name="row_attention",
    )(place, *pieces, halo)


def near_kernel(
    z_ref, cos_ref, sin_ref, pcos_ref, psin_ref, q_hbm, k_hbm, v_hbm, halo_ref, out_ref, log_ref, q_ref, k_ref, v_ref, sem
):
    pairs = ((q_hbm, q_ref), (k_hbm, k_ref), (v_hbm, v_ref))
    copies = [pltpu.make_async_copy(a.at[0], b, sem.at[i]) for i, (a, b) in enumerate(pairs)]
    for copy in copies:
        copy.start()
    bias = jnp.where(z_ref[0] == 0, MASKED, -MASKED)
    cosine, sine = full_tables(cos_ref, sin_ref)
    pcos, psin = full_tables(pcos_ref, psin_ref)
    lane = iota((TOKENS, HEAD), 1)

    held = jnp.zeros((TOKENS, HEAD), f32)
    for copy in copies:
        copy.wait()
    for h in range(LOCAL):
        lanes = slice(h * HEAD, (h + 1) * HEAD)
        q = (turned(q_ref[:, lanes], cosine, sine) * SCALE).astype(bf16)
        k = turned(k_ref[:, lanes], cosine, sine).astype(bf16)
        v = v_ref[:, lanes]
        ks = [turned(halo_ref[0, :, lanes], pcos, psin).astype(bf16), k[:HALF], k[HALF:]]
        vs = [halo_ref[1, :, lanes], v[:HALF], v[HALF:]]
        parts = []
        for b in range(2):
            result, logs = attend(
                q[b * HALF : (b + 1) * HALF], ks[b], ks[b + 1], vs[b], vs[b + 1], bias if b == 0 else None
            )
            out_ref[b * HALF : (b + 1) * HALF, lanes] = result.astype(bf16)
            parts.append(wide(logs))
        held = jnp.where(lane == h, jnp.concatenate(parts, axis=0), held)
    log_ref[...] = held


def near_attention(device, cosine, sine, pcos, psin, queries, keys, values, halo):
    vmem, hbm = pl.BlockSpec(memory_space=pltpu.VMEM), pl.BlockSpec(memory_space=pltpu.HBM)
    return pl.pallas_call(
        near_kernel,
        in_specs=[pl.BlockSpec(memory_space=pltpu.SMEM)] + [vmem] * 4 + [hbm] * 3 + [vmem],
        out_specs=[vmem] * 2,
        out_shape=[
            jax.ShapeDtypeStruct((TOKENS, LOCAL * HEAD), bf16),
            jax.ShapeDtypeStruct((TOKENS, HEAD), f32),
        ],
        scratch_shapes=[pltpu.VMEM((TOKENS, LOCAL * HEAD), bf16)] * 3 + [pltpu.SemaphoreType.DMA((3,))],
        cost_estimate=pl.CostEstimate(flops=2**31, bytes_accessed=4 * 2**20, transcendentals=2**19),
        name="near_attention",
    )(device, cosine, sine, pcos, psin, queries, keys, values, halo)


def merge_kernel(x_ref, near_ref, log_ref, far_ref, own_ref, one_ref, two_ref, three_ref, out_ref, far, far_log, mid, mid_log, row_ref):
    x = x_ref[0]
    for steps, ref in enumerate((own_ref, one_ref, two_ref, three_ref)):
        row_ref[lax.rem(x + ROW - steps, ROW)] = ref[...]
    for h in range(LOCAL):
        lanes = slice(h * HEAD, (h + 1) * HEAD)
        for p in range(2):
            piece = 2 * h + p
            logs = rows_to_column(far_ref[piece, HALF : HALF + 1, :], far_ref[piece, HALF + 1 : HALF + 2, :])
            for r in range(8):
                target = pl.ds(p + 2 * r, 16, stride=16)
                far[h % 2, target, :] = far_ref[piece, r * 16 : (r + 1) * 16, :].astype(f32)
                far_log[h % 2, target, :] = logs[r * 16 : (r + 1) * 16]
        chip, head = h // ROW_HEADS, h % ROW_HEADS
        for half in range(2):
            rows = TOKENS + 2 * half
            logs = rows_to_column(row_ref[chip, head, rows : rows + 1, :], row_ref[chip, head, rows + 1 : rows + 2, :])
            for i in range(2):
                r = 2 * half + i
                target = pl.ds(r, 64, stride=4)
                mid[h % 2, target, :] = row_ref[chip, head, r * 64 : (r + 1) * 64, :].astype(f32)
                mid_log[h % 2, target, :] = logs[i * 64 : (i + 1) * 64]
        logs = [wide(log_ref[:, h : h + 1]), mid_log[h % 2], far_log[h % 2]]
        top = jnp.maximum(jnp.maximum(logs[0], logs[1]), logs[2])
        e = [jnp.exp(x - top) for x in logs]
        total = e[0] * near_ref[:, lanes].astype(f32) + e[1] * mid[h % 2] + e[2] * far[h % 2]
        out_ref[:, lanes] = (total / (e[0] + e[1] + e[2])).astype(bf16)


def merge_groups(x, near, log, far, own, others):

    vmem = pl.BlockSpec(memory_space=pltpu.VMEM)
    return pl.pallas_call(
        merge_kernel,
        in_specs=[pl.BlockSpec(memory_space=pltpu.SMEM)] + [vmem] * 7,
        out_specs=vmem,
        out_shape=jax.ShapeDtypeStruct((TOKENS, LOCAL * HEAD), bf16),
        scratch_shapes=[pltpu.VMEM((2, TOKENS, HEAD), f32)] * 4 + [pltpu.VMEM((ROW, *own.shape), bf16)],
        compiler_params=pltpu.CompilerParams(vmem_limit_bytes=8 * 2**20),
        cost_estimate=pl.CostEstimate(flops=2**24, bytes_accessed=2**21, transcendentals=2**19),
        name="merge_groups",
    )(x, near, log, far, own, *others)


def project_kernel(core_ref, mine_ref, other_ref, w_ref, out_ref):
    half = LOCAL * HEAD
    core = core_ref[0]
    mine = pl.ds(pl.multiple_of(core * half, half), half)
    other = pl.ds(pl.multiple_of((1 - core) * half, half), half)
    total = jnp.dot(mine_ref[...], w_ref[mine, :], preferred_element_type=f32)
    total += jnp.dot(other_ref[...], w_ref[other, :], preferred_element_type=f32)
    out_ref[...] = total.astype(bf16)


def project(core, mine, other, w_out):
    vmem = pl.BlockSpec(memory_space=pltpu.VMEM)
    return pl.pallas_call(
        project_kernel,
        in_specs=[pl.BlockSpec(memory_space=pltpu.SMEM), vmem, vmem, vmem],
        out_specs=vmem,
        out_shape=jax.ShapeDtypeStruct((TOKENS, w_out.shape[1]), bf16),
        compiler_params=pltpu.CompilerParams(vmem_limit_bytes=8 * 2**20),
        cost_estimate=pl.CostEstimate(flops=2**30, bytes_accessed=2**22, transcendentals=0),
        name="project",
    )(core, mine, other, w_out)


def tables(count, start):
    inverse = ROPE_BASE ** (-jnp.arange(0, HEAD, 2, dtype=f32) / HEAD)
    angles = (lax.iota(jnp.int32, count) + start).astype(f32)[:, None] * inverse[None, :]
    return jnp.cos(angles), jnp.sin(angles)


def shards(queries, keys, values, w_out):
    devices = lax.axis_size("sp")
    assert queries.shape == (3, TOKENS, LOCAL * HEAD) and devices % PLANE == 0
    planes = [[p * PLANE + i for i in range(PLANE)] for p in range(devices // PLANE)]
    exchange = functools.partial(
        lax.all_to_all, axis_name="sp", split_axis=0, concat_axis=0, axis_index_groups=planes, tiled=True
    )

    def along_row(block, steps):
        return lax.ppermute(block, "sp", [(i, i // ROW * ROW + (i + steps) % ROW) for i in range(devices)])

    def onward(block, distance):
        return lax.ppermute(block, "sp", [(i, i + distance) for i in range(devices - distance)])

    device = lax.axis_index("sp")
    core = lax.axis_index("tp").reshape(1)
    x = lax.rem(device, ROW).reshape(1)
    start = device * TOKENS
    cosine, sine = tables(TOKENS, start)

    edge = onward(jnp.stack([keys[0, HALF:], values[0, HALF:]]), 1)
    held = plane_pieces(keys, values, queries, cosine, sine)
    held = exchange(held)
    own, *others = row_pieces(x, keys, values, queries, cosine, sine)
    pieces = [own] + [along_row(block, steps) for steps, block in enumerate(others, 1)]
    halo2 = onward(held[PLANE // 2 :, :2], PLANE)
    last = pick_last(x, pieces)
    halo1 = onward(last, ROW)
    pcos, psin = tables(HALF, start - HALF)
    near, log = near_attention(device.reshape(1), cosine, sine, pcos, psin, queries, keys, values, edge)
    far = plane_attention((device // PLANE).reshape(1), held, halo2)
    far = exchange(far)
    mine, *sent = row_attention(jnp.stack([x[0], device // ROW]), pieces, halo1)
    back = [along_row(block, steps) for steps, block in enumerate(sent, 1)]
    attended = merge_groups(x, near, log, far, mine, back)
    other = lax.ppermute(attended, "tp", [(0, 1), (1, 0)])
    return project(core, attended, other, w_out)


def solution(mesh):
    return jax.shard_map(
        shards,
        mesh=mesh,
        in_specs=(P(None, "sp", "tp"), P(None, "sp", "tp"), P(None, "sp", "tp"), P(None, "tp")),
        out_specs=P("sp", "tp"),
        check_vma=False,
    )
```

profile of v0, /device:TPU:9, one launch (start us, length us, event | category | flops | bytes accessed | tf_op | source)
XLA Modules:
  0.0 116.3 jit_solution(13057423865799710661)
XLA Ops:
  0.0 1.3 %multiply_sine_fusion = (f32[256,64]{1,0:T(8,128)}, f32[256,64]{1,0:T(8,128)}) fusion(f32[64]{0:T(128)S(1)} %multiply_power_fusion, f32[256]{0:T(256)S(1)} %add_convert_fusion), kind=kLoop, calls=%fused_computation.1 | loop fusion | flops 16384 | bytes 132352 | tf_op jit(solution)/shard_map/sin | solution.py:409
  1.3 4.5 %plane_pieces.1 = bf16[16,3,128,128]{3,2,1,0:T(8,128)(2,1)} custom-call(f32[256,64]{1,0:T(8,128)} %get-tuple-element.26.cos_ref, f32[256,64]{1,0:T(8,128)} %get-tuple-element.25.sin_ref, bf16[3,256,1024]{2,1,0:T(8,128)(2,1)} %k_ref.3, bf16[3,256,1024]{2,1,0:T(8,128)(2,1)} %v_ref.3, bf16[3,256,1024]{2,1,0:T(8,128)(2,1)} %q_ref.3), custom_call_target="tpu_custom_call" | custom-call | flops 1073741824 | bytes 3145728 | tf_op jit(solution)/shard_map/plane_pieces/pallas_call | solution.py:78
  5.7 26.8 %all_to_all.10.in_ref = bf16[16,3,128,128]{3,2,1,0:T(8,128)(2,1)S(1)} all-to-all(bf16[16,3,128,128]{3,2,1,0:T(8,128)(2,1)} %plane_pieces.1), channel_id=1, replica_groups={{0,2,4,6,8,10,12,14,16,18,20,22,24,26,28,30},{32,34,36,38,40,42,44,46,4..., dimensions={0} | all-to-all | bytes 3145728 | tf_op jit(solution)/shard_map/all_to_all | solution.py:434
  32.5 0.8 slice.12
  33.4 4.3 %collective-permute-start.1 = (bf16[8,2,128,128]{3,2,1,0:T(8,128)(2,1)}, bf16[8,2,128,128]{3,2,1,0:T(8,128)(2,1)}, u32[]{:S(2)}, u32[]{:S(2)}) collective-permute-start(bf16[8,2,128,128]{3,2,1,0:T(8,128)(2,1)} %slice.12), channel_id=1, source_target_pairs={{0,32},{2,34},{4,36},{6,38},{8,40},{10,42},{12,44},{14,46},{16,48}... | collective-permute-start | bytes 1572872 | tf_op jit(solution)/shard_map/ppermute | solution.py:424
  37.7 3.7 %row_pieces.1 = (bf16[3,2,256,128]{3,2,1,0:T(8,128)(2,1)}, bf16[3,2,256,128]{3,2,1,0:T(8,128)(2,1)}, bf16[3,2,256,128]{3,2,1,0:T(8,128)(2,1)}, bf16[3,2,256,128]{3,2,1,0:T(8,128)(2,1)}) custom-call(s32[1]{0:T(128)} %bitcast.1.x_ref, f32[256,64]{1,0:T(8,128)} %get-tuple-element.26.cos_ref, f32[256,64]{1,0:T(8,128)} %get-tuple-element.25.sin_ref, ...), custom_call_target="tpu_custom_call" | custom-call | flops 1073741824 | bytes 3145728 | tf_op jit(solution)/shard_map/row_pieces/pallas_call | solution.py:124
  41.5 0.0 copy-start.2
  41.5 0.1 collective-permute-start.2
  41.6 1.8 %collective-permute-start.3 = (bf16[3,2,256,128]{3,2,1,0:T(8,128)(2,1)}, bf16[3,2,256,128]{3,2,1,0:T(8,128)(2,1)S(1)}, u32[]{:S(2)}, u32[]{:S(2)}) collective-permute-start(bf16[3,2,256,128]{3,2,1,0:T(8,128)(2,1)} %get-tuple-element.19), channel_id=1, source_target_pairs={{0,4},{2,6},{4,0},{6,2},{8,12},{10,14},{12,8},{14,10},{16,20},{18,... | collective-permute-start | bytes 1179656 | tf_op jit(solution)/shard_map/ppermute | solution.py:421
  43.3 1.8 %collective-permute-start.4 = (bf16[3,2,256,128]{3,2,1,0:T(8,128)(2,1)}, bf16[3,2,256,128]{3,2,1,0:T(8,128)(2,1)S(1)}, u32[]{:S(2)}, u32[]{:S(2)}) collective-permute-start(bf16[3,2,256,128]{3,2,1,0:T(8,128)(2,1)} %get-tuple-element.20), channel_id=1, source_target_pairs={{0,6},{2,0},{4,2},{6,4},{8,14},{10,8},{12,10},{14,12},{16,22},{18,... | collective-permute-start | bytes 1179656 | tf_op jit(solution)/shard_map/ppermute | solution.py:421
  45.1 1.0 slice.10
  46.1 1.0 slice.9
  47.1 0.8 pad_maximum_fusion
  47.9 1.9 %collective-permute-start = (bf16[2,128,1024]{2,1,0:T(8,128)(2,1)}, bf16[2,128,1024]{2,1,0:T(8,128)(2,1)}, u32[]{:S(2)}, u32[]{:S(2)}) collective-permute-start(bf16[2,128,1024]{2,1,0:T(8,128)(2,1)} %pad_maximum_fusion), channel_id=1, source_target_pairs={{0,2},{2,4},{4,6},{6,8},{8,10},{10,12},{12,14},{14,16},{16,18},{18... | collective-permute-start | bytes 1572872 | tf_op jit(solution)/shard_map/ppermute | solution.py:424
  49.9 3.6 %collective-permute-done.2.one_ref.refs_1_ = bf16[3,2,256,128]{3,2,1,0:T(8,128)(2,1)S(1)} collective-permute-done((bf16[3,2,256,128]{3,2,1,0:T(8,128)(2,1)}, bf16[3,2,256,128]{3,2,1,0:T(8,128)(2,1)S(1)}, u32[]{:S(2)}, u32[]{:S(2)}) %collective-permute-start.2) | collective-permute-done | bytes 393248 | tf_op jit(solution)/shard_map/ppermute | solution.py:421
  53.5 5.3 %collective-permute-done.3.two_ref.refs_2_ = bf16[3,2,256,128]{3,2,1,0:T(8,128)(2,1)S(1)} collective-permute-done((bf16[3,2,256,128]{3,2,1,0:T(8,128)(2,1)}, bf16[3,2,256,128]{3,2,1,0:T(8,128)(2,1)S(1)}, u32[]{:S(2)}, u32[]{:S(2)}) %collective-permute-start.3) | collective-permute-done | bytes 393248 | tf_op jit(solution)/shard_map/ppermute | solution.py:421
  58.8 3.3 %collective-permute-done.4.three_ref.refs_3_ = bf16[3,2,256,128]{3,2,1,0:T(8,128)(2,1)S(1)} collective-permute-done((bf16[3,2,256,128]{3,2,1,0:T(8,128)(2,1)}, bf16[3,2,256,128]{3,2,1,0:T(8,128)(2,1)S(1)}, u32[]{:S(2)}, u32[]{:S(2)}) %collective-permute-start.4) | collective-permute-done | bytes 393248 | tf_op jit(solution)/shard_map/ppermute | solution.py:421
  62.1 0.0 copy-start.3
  62.1 0.7 copy-done.3
  62.8 0.0 copy-done.2
  62.8 0.0 copy-start.4
  62.8 1.0 copy-done.4
  63.9 3.1 %collective-permute-start.5 = (bf16[2,2,2,256,128]{4,3,2,1,0:T(8,128)(2,1)S(1)}, bf16[2,2,2,256,128]{4,3,2,1,0:T(8,128)(2,1)}, u32[]{:S(2)}, u32[]{:S(2)}) collective-permute-start(bf16[2,2,2,256,128]{4,3,2,1,0:T(8,128)(2,1)S(1)} %pick_last.1), channel_id=1, source_target_pairs={{0,8},{2,10},{4,12},{6,14},{8,16},{10,18},{12,20},{14,22},{16,24},... | collective-permute-start | bytes 1572872 | tf_op jit(solution)/shard_map/ppermute | solution.py:424
  67.0 0.0 collective-permute-done.1.halo_ref
  67.0 3.6 %plane_attention.1 = bf16[16,144,128]{2,1,0:T(8,128)(2,1)} custom-call(s32[1]{0:T(128)} %bitcast.3.z_ref, bf16[16,3,128,128]{3,2,1,0:T(8,128)(2,1)S(1)} %all_to_all.10.in_ref, bf16[8,2,128,128]{3,2,1,0:T(8,128)(2,1)} %collective-permute-done.1.halo_ref), custom_call_target="tpu_custom_call" | custom-call | flops 2147483648 | bytes 3145728 | tf_op jit(solution)/shard_map/plane_attention/pallas_call | solution.py:206
  70.6 7.8 %all-to-all-start.1 = ((bf16[16,144,128]{2,1,0:T(8,128)(2,1)}), bf16[16,144,128]{2,1,0:T(8,128)(2,1)S(1)}, u32[]{:S(2)}, u32[]{:S(2)}) async-start(bf16[16,144,128]{2,1,0:T(8,128)(2,1)} %plane_attention.1), calls=%async_computation.1 | async-start | bytes 1179648 | tf_op jit(solution)/shard_map/all_to_all | solution.py:443
  78.5 1.0 multiply_sine_fusion.1
  79.4 0.1 pad_add_fusion.x_ref
  79.5 11.8 %collective-permute-done.5.refs_4_ = bf16[2,2,2,256,128]{4,3,2,1,0:T(8,128)(2,1)} collective-permute-done((bf16[2,2,2,256,128]{4,3,2,1,0:T(8,128)(2,1)S(1)}, bf16[2,2,2,256,128]{4,3,2,1,0:T(8,128)(2,1)}, u32[]{:S(2)}, u32[]{:S(2)}) %collective-permute-start.5) | collective-permute-done | bytes 524320 | tf_op jit(solution)/shard_map/ppermute | solution.py:424
  91.3 0.0 copy-start.5
  91.3 1.0 copy-done.5
  92.3 3.4 %row_attention.1 = (bf16[2,272,128]{2,1,0:T(8,128)(2,1)S(1)}, bf16[2,272,128]{2,1,0:T(8,128)(2,1)S(1)}, bf16[2,272,128]{2,1,0:T(8,128)(2,1)S(1)}, bf16[2,272,128]{2,1,0:T(8,128)(2,1)S(1)}) custom-call(s32[2]{0:T(128)S(1)} %pad_add_fusion.x_ref, bf16[3,2,256,128]{3,2,1,0:T(8,128)(2,1)S(1)} %copy-done.2, ...), custom_call_target="tpu_custom_call" | custom-call | flops 2147483648 | bytes 3145728 | tf_op jit(solution)/shard_map/row_attention/pallas_call | solution.py:274
  95.7 0.1 collective-permute-start.6
  95.8 0.1 collective-permute-start.7
  95.9 2.6 %collective-permute-start.8 = (bf16[2,272,128]{2,1,0:T(8,128)(2,1)S(1)}, bf16[2,272,128]{2,1,0:T(8,128)(2,1)S(1)}, u32[]{:S(2)}, u32[]{:S(2)}) collective-permute-start(bf16[2,272,128]{2,1,0:T(8,128)(2,1)S(1)} %get-tuple-element.24), channel_id=1, source_target_pairs={{0,6},{2,0},{4,2},{6,4},{8,14},{10,8},{12,10},{14,12},{16,22},{18,... | collective-permute-start | bytes 417800 | tf_op jit(solution)/shard_map/ppermute | solution.py:421
  98.5 0.0 collective-permute-done.halo_ref
  98.5 5.7 %near_attention.1 = (bf16[256,1024]{1,0:T(8,128)(2,1)}, f32[256,128]{1,0:T(8,128)}) custom-call(s32[1]{0:T(128)} %bitcast.2.z_ref, f32[256,64]{1,0:T(8,128)} %get-tuple-element.26.cos_ref, f32[256,64]{1,0:T(8,128)} %get-tuple-element.25.sin_ref, f32[128,64]{1,0:T(8,128)} %get-tuple-element.28.pcos_ref, f32[128,64]{1,0:T(8,128)} %get-tuple-element.27.psin_ref, ...), custom_call_target="tpu_custom_call" | custom-call | flops 2147483648 | bytes 4194304 | tf_op jit(solution)/shard_map/near_attention/pallas_call | solution.py:325
  104.1 1.0 collective-permute-done.6.one_ref
  105.2 0.0 collective-permute-done.7.two_ref
  105.2 0.0 collective-permute-done.8.three_ref
  105.2 0.0 all-to-all-done.1.far_ref
  105.2 0.0 copy-start.1
  105.2 1.0 copy-done.1
  106.2 0.0 copy-start.6
  106.2 0.9 copy-done.6
  107.1 1.8 %merge_groups.1.mine_ref = bf16[256,1024]{1,0:T(8,128)(2,1)S(1)} custom-call(s32[1]{0:T(128)} %bitcast.1.x_ref, bf16[256,1024]{1,0:T(8,128)(2,1)S(1)} %copy-done.1, f32[256,128]{1,0:T(8,128)S(1)} %copy-done.6, bf16[16,144,128]{2,1,0:T(8,128)(2,1)S(1)} %all-to-all-done.1.far_ref, bf16[2,272,128]{2,1,0:T(8,128)(2,1)S(1)} %get-tuple-element.21.own_ref, ...), custom_call_target="tpu_custom_call" | custom-call | flops 16777216 | bytes 2097152 | tf_op jit(solution)/shard_map/merge_groups/pallas_call | solution.py:371
  109.0 1.6 %collective-permute-start.9 = (bf16[256,1024]{1,0:T(8,128)(2,1)S(1)}, bf16[256,1024]{1,0:T(8,128)(2,1)S(1)}, u32[]{:S(2)}, u32[]{:S(2)}) collective-permute-start(bf16[256,1024]{1,0:T(8,128)(2,1)S(1)} %merge_groups.1.mine_ref), channel_id=1, source_target_pairs={{0,1},{1,0},{2,3},{3,2},{4,5},{5,4},{6,7},{7,6},{8,9},{9,8},{10,11... | collective-permute-start | bytes 1572872 | tf_op jit(solution)/shard_map/ppermute | solution.py:447
  110.6 1.5 %collective-permute-done.9.other_ref = bf16[256,1024]{1,0:T(8,128)(2,1)S(1)} collective-permute-done((bf16[256,1024]{1,0:T(8,128)(2,1)S(1)}, bf16[256,1024]{1,0:T(8,128)(2,1)S(1)}, u32[]{:S(2)}, u32[]{:S(2)}) %collective-permute-start.9) | collective-permute-done | bytes 524320 | tf_op jit(solution)/shard_map/ppermute | solution.py:447
  112.1 0.0 copy-start
  112.1 2.2 %copy-done = bf16[2048,1024]{1,0:T(8,128)(2,1)S(1)} copy-done((bf16[2048,1024]{1,0:T(8,128)(2,1)S(1)}, bf16[2048,1024]{1,0:T(8,128)(2,1)}, u32[]{:S(2)}) %copy-start) | copy-done | bytes 4194328
  114.3 2.1 %project.1 = bf16[256,1024]{1,0:T(8,128)(2,1)} custom-call(s32[1]{0:T(128)} %bitcast.core_ref, bf16[256,1024]{1,0:T(8,128)(2,1)S(1)} %merge_groups.1.mine_ref, bf16[256,1024]{1,0:T(8,128)(2,1)S(1)} %collective-permute-done.9.other_ref, bf16[2048,1024]{1,0:T(8,128)(2,1)S(1)} %copy-done), custom_call_target="tpu_custom_call" | custom-call | flops 1073741824 | bytes 4194304 | tf_op jit(solution)/shard_map/project/pallas_call | solution.py:395
  (4 shorter events, 0.1 us)
Async XLA Ops:
  33.4 33.6 %collective-permute-start.1 = (bf16[8,2,128,128]{3,2,1,0:T(8,128)(2,1)}, bf16[8,2,128,128]{3,2,1,0:T(8,128)(2,1)}, u32[]{:S(2)}, u32[]{:S(2)}) collective-permute-start(bf16[8,2,128,128]{3,2,1,0:T(8,128)(2,1)} %slice.12), channel_id=1, source_target_pairs={{0,32},{2,34},{4,36},{6,38},{8,40},{10,42},{12,44},{14,46},{16,48}... | collective-permute-start | bytes 1572872 | tf_op jit(solution)/shard_map/ppermute | solution.py:424
  41.5 21.4 %copy-start.2 = (bf16[3,2,256,128]{3,2,1,0:T(8,128)(2,1)S(1)}, bf16[3,2,256,128]{3,2,1,0:T(8,128)(2,1)}, u32[]{:S(2)}) copy-start(bf16[3,2,256,128]{3,2,1,0:T(8,128)(2,1)} %get-tuple-element.17.own_ref.refs_0_) | copy-start | bytes 1179652
  41.5 12.0 %collective-permute-start.2 = (bf16[3,2,256,128]{3,2,1,0:T(8,128)(2,1)}, bf16[3,2,256,128]{3,2,1,0:T(8,128)(2,1)S(1)}, u32[]{:S(2)}, u32[]{:S(2)}) collective-permute-start(bf16[3,2,256,128]{3,2,1,0:T(8,128)(2,1)} %get-tuple-element.18), channel_id=1, source_target_pairs={{0,2},{2,4},{4,6},{6,0},{8,10},{10,12},{12,14},{14,8},{16,18},{18,... | collective-permute-start | bytes 1179656 | tf_op jit(solution)/shard_map/ppermute | solution.py:421
  41.6 17.2 %collective-permute-start.3 = (bf16[3,2,256,128]{3,2,1,0:T(8,128)(2,1)}, bf16[3,2,256,128]{3,2,1,0:T(8,128)(2,1)S(1)}, u32[]{:S(2)}, u32[]{:S(2)}) collective-permute-start(bf16[3,2,256,128]{3,2,1,0:T(8,128)(2,1)} %get-tuple-element.19), channel_id=1, source_target_pairs={{0,4},{2,6},{4,0},{6,2},{8,12},{10,14},{12,8},{14,10},{16,20},{18,... | collective-permute-start | bytes 1179656 | tf_op jit(solution)/shard_map/ppermute | solution.py:421
  43.3 18.8 %collective-permute-start.4 = (bf16[3,2,256,128]{3,2,1,0:T(8,128)(2,1)}, bf16[3,2,256,128]{3,2,1,0:T(8,128)(2,1)S(1)}, u32[]{:S(2)}, u32[]{:S(2)}) collective-permute-start(bf16[3,2,256,128]{3,2,1,0:T(8,128)(2,1)} %get-tuple-element.20), channel_id=1, source_target_pairs={{0,6},{2,0},{4,2},{6,4},{8,14},{10,8},{12,10},{14,12},{16,22},{18,... | collective-permute-start | bytes 1179656 | tf_op jit(solution)/shard_map/ppermute | solution.py:421
  47.9 50.5 %collective-permute-start = (bf16[2,128,1024]{2,1,0:T(8,128)(2,1)}, bf16[2,128,1024]{2,1,0:T(8,128)(2,1)}, u32[]{:S(2)}, u32[]{:S(2)}) collective-permute-start(bf16[2,128,1024]{2,1,0:T(8,128)(2,1)} %pad_maximum_fusion), channel_id=1, source_target_pairs={{0,2},{2,4},{4,6},{6,8},{8,10},{10,12},{12,14},{14,16},{16,18},{18... | collective-permute-start | bytes 1572872 | tf_op jit(solution)/shard_map/ppermute | solution.py:424
  62.1 0.7 copy-start.3
  62.8 1.0 copy-start.4
  63.9 27.4 %collective-permute-start.5 = (bf16[2,2,2,256,128]{4,3,2,1,0:T(8,128)(2,1)S(1)}, bf16[2,2,2,256,128]{4,3,2,1,0:T(8,128)(2,1)}, u32[]{:S(2)}, u32[]{:S(2)}) collective-permute-start(bf16[2,2,2,256,128]{4,3,2,1,0:T(8,128)(2,1)S(1)} %pick_last.1), channel_id=1, source_target_pairs={{0,8},{2,10},{4,12},{6,14},{8,16},{10,18},{12,20},{14,22},{16,24},... | collective-permute-start | bytes 1572872 | tf_op jit(solution)/shard_map/ppermute | solution.py:424
  70.6 34.6 %all-to-all-start.1 = ((bf16[16,144,128]{2,1,0:T(8,128)(2,1)}), bf16[16,144,128]{2,1,0:T(8,128)(2,1)S(1)}, u32[]{:S(2)}, u32[]{:S(2)}) async-start(bf16[16,144,128]{2,1,0:T(8,128)(2,1)} %plane_attention.1), calls=%async_computation.1 | async-start | bytes 1179648 | tf_op jit(solution)/shard_map/all_to_all | solution.py:443
  91.3 1.0 copy-start.5
  95.7 9.5 %collective-permute-start.6 = (bf16[2,272,128]{2,1,0:T(8,128)(2,1)S(1)}, bf16[2,272,128]{2,1,0:T(8,128)(2,1)S(1)}, u32[]{:S(2)}, u32[]{:S(2)}) collective-permute-start(bf16[2,272,128]{2,1,0:T(8,128)(2,1)S(1)} %get-tuple-element.22), channel_id=1, source_target_pairs={{0,2},{2,4},{4,6},{6,0},{8,10},{10,12},{12,14},{14,8},{16,18},{18,... | collective-permute-start | bytes 417800 | tf_op jit(solution)/shard_map/ppermute | solution.py:421
  95.8 9.4 %collective-permute-start.7 = (bf16[2,272,128]{2,1,0:T(8,128)(2,1)S(1)}, bf16[2,272,128]{2,1,0:T(8,128)(2,1)S(1)}, u32[]{:S(2)}, u32[]{:S(2)}) collective-permute-start(bf16[2,272,128]{2,1,0:T(8,128)(2,1)S(1)} %get-tuple-element.23), channel_id=1, source_target_pairs={{0,4},{2,6},{4,0},{6,2},{8,12},{10,14},{12,8},{14,10},{16,20},{18,... | collective-permute-start | bytes 417800 | tf_op jit(solution)/shard_map/ppermute | solution.py:421
  95.9 9.3 %collective-permute-start.8 = (bf16[2,272,128]{2,1,0:T(8,128)(2,1)S(1)}, bf16[2,272,128]{2,1,0:T(8,128)(2,1)S(1)}, u32[]{:S(2)}, u32[]{:S(2)}) collective-permute-start(bf16[2,272,128]{2,1,0:T(8,128)(2,1)S(1)} %get-tuple-element.24), channel_id=1, source_target_pairs={{0,6},{2,0},{4,2},{6,4},{8,14},{10,8},{12,10},{14,12},{16,22},{18,... | collective-permute-start | bytes 417800 | tf_op jit(solution)/shard_map/ppermute | solution.py:421
  105.2 1.0 copy-start.1
  106.2 0.9 copy-start.6
  109.0 3.1 %collective-permute-start.9 = (bf16[256,1024]{1,0:T(8,128)(2,1)S(1)}, bf16[256,1024]{1,0:T(8,128)(2,1)S(1)}, u32[]{:S(2)}, u32[]{:S(2)}) collective-permute-start(bf16[256,1024]{1,0:T(8,128)(2,1)S(1)} %merge_groups.1.mine_ref), channel_id=1, source_target_pairs={{0,1},{1,0},{2,3},{3,2},{4,5},{5,4},{6,7},{7,6},{8,9},{9,8},{10,11... | collective-permute-start | bytes 1572872 | tf_op jit(solution)/shard_map/ppermute | solution.py:447
  112.1 2.2 %copy-start = (bf16[2048,1024]{1,0:T(8,128)(2,1)S(1)}, bf16[2048,1024]{1,0:T(8,128)(2,1)}, u32[]{:S(2)}) copy-start(bf16[2048,1024]{1,0:T(8,128)(2,1)} %w_ref.1) | copy-start | bytes 12582916
where the time goes:
time: 117 us; the launch traced here: 116 us
  blocking collectives  26.8 us (23%)
  waiting for transfers between devices  26.6 us (23%)
  starting transfers between devices  25.2 us (22%)
  Pallas kernels  24.8 us (21%)
  local copies, waits for them, and re-layouts  9.64 us (8%)
  other arithmetic  3.15 us (3%)
    all_to_all x1, blocking collectives, shards(): held = exchange(held)  26.8 us
    ppermute x6, waiting for transfers between devices, along_row(): lax.ppermute(block, 'sp', [(i, i // ROW * ROW + (i + steps) % ROW) for i...  13.3 us
    ppermute x3, waiting for transfers between devices, onward(): lax.ppermute(block, 'sp', [(i, i + distance) for i in range(devices - dis...  11.8 us
    ppermute x3, starting transfers between devices, onward(): lax.ppermute(block, 'sp', [(i, i + distance) for i in range(devices - dis...  9.34 us
    all_to_all x1, starting transfers between devices, shards(): far = exchange(far)  7.84 us
    unnamed x14, local copies, waits for them, and re-layouts  6.86 us
    ppermute x6, starting transfers between devices, along_row(): lax.ppermute(block, 'sp', [(i, i // ROW * ROW + (i + steps) % ROW) for i...  6.39 us
    pallas_call x1, Pallas kernels, near_attention(): pl.pallas_call(near_kernel, in_specs=[pl.BlockSpec(memory_space=pltpu.SME...  5.67 us
  transfers between devices with their start and end apart: 11, of which 6 were waited for; matrix products, arithmetic and copies ran while one was open for 3% of the time, Pallas kernels for 14%

commit v1 on v0

--- a/solution.py
+++ b/solution.py
@@ -93,8 +93,8 @@
 
 
 def row_pieces_kernel(x_ref, cos_ref, sin_ref, k_ref, v_ref, q_ref, *refs):
-    outs = refs[:ROW]
-    in_ref, sort_ref, piece_ref, sem, out_sem = refs[ROW:]
+    outs, q_outs = refs[:ROW], refs[ROW : 2 * ROW]
+    in_ref, sort_ref, piece_ref, sem, out_sem = refs[2 * ROW :]
     copies = fetched([ref.at[1] for ref in (k_ref, v_ref, q_ref)], in_ref, sem)
     cosine, sine = full_tables(cos_ref, sin_ref)
     stores = []
@@ -113,7 +113,7 @@
                 sort_ref[slot] = turned_as(kind, in_ref[a, :, lanes], cosine, sine)
                 rows = [sort_ref[slot, pl.ds(r, 64, stride=4), :] for r in range(4)]
                 piece_ref[steps, a, h] = jnp.concatenate(rows, axis=0).astype(bf16)
-            store(piece_ref.at[steps, a], outs[steps].at[a], a * ROW + steps)
+            store(piece_ref.at[steps, a], q_outs[steps] if kind == "q" else outs[steps].at[a], a * ROW + steps)
     for copy in stores:
         copy.wait()
 
@@ -121,10 +121,10 @@
 def row_pieces(x, keys, values, queries, cosine, sine):
     vmem, hbm = pl.BlockSpec(memory_space=pltpu.VMEM), pl.BlockSpec(memory_space=pltpu.HBM)
     shape = (ROW_HEADS, TOKENS, HEAD)
-    return pl.pallas_call(
+    outs = pl.pallas_call(
         row_pieces_kernel,
         in_specs=[pl.BlockSpec(memory_space=pltpu.SMEM), vmem, vmem, hbm, hbm, hbm],
-        out_specs=[hbm] * ROW,
+        out_specs=[hbm] * (2 * ROW),
         scratch_shapes=[
             pltpu.VMEM((3, TOKENS, LOCAL * HEAD), bf16),
             pltpu.VMEM((LOCAL, TOKENS, HEAD), f32),
@@ -132,10 +132,11 @@
             pltpu.SemaphoreType.DMA((3,)),
             pltpu.SemaphoreType.DMA((3 * ROW,)),
         ],
-        out_shape=[jax.ShapeDtypeStruct((3, *shape), bf16)] * ROW,
+        out_shape=[jax.ShapeDtypeStruct((2, *shape), bf16)] * ROW + [jax.ShapeDtypeStruct(shape, bf16)] * ROW,
         cost_estimate=pl.CostEstimate(flops=2**30, bytes_accessed=3 * 2**20, transcendentals=0),
         name="row_pieces",
     )(x, cosine, sine, keys, values, queries)
+    return list(outs[:ROW]), list(outs[ROW:])
 
 
 def dot_t(a, b):
@@ -222,7 +223,7 @@
 
         @pl.when(chip >= ROW // 2)
         def _(ref=ref, chip=chip):
-            out_ref[chip - ROW // 2] = ref[:2]
+            out_ref[chip - ROW // 2] = ref[...]
 
 
 def pick_last(x, pieces):
@@ -239,12 +240,14 @@
 
 
 def row_kernel(x_ref, *refs):
-    ins, halo_ref, outs = refs[:ROW], refs[ROW], refs[ROW + 1 : 2 * ROW + 1]
-    in_ref, res_ref, logs_ref = refs[2 * ROW + 1 :]
+    ins, q_ins, halo_ref, outs = refs[:ROW], refs[ROW : 2 * ROW], refs[2 * ROW], refs[2 * ROW + 1 : 3 * ROW + 1]
+    in_ref, q_ref, res_ref, logs_ref = refs[3 * ROW + 1 :]
     x = x_ref[0]
     bias = jnp.where(x_ref[1] == 0, MASKED, -MASKED)
     for steps in range(ROW):
-        in_ref[lax.rem(x + ROW - steps, ROW)] = ins[steps][...]
+        chip = lax.rem(x + ROW - steps, ROW)
+        in_ref[chip] = ins[steps][...]
+        q_ref[chip] = q_ins[steps][...]
     for h in range(ROW_HEADS):
         for r in range(4):
             rows = slice(r * 64, (r + 1) * 64)
@@ -254,7 +257,7 @@
                 chips = (2 * b, 2 * b + 1)
                 ks.append(jnp.concatenate([in_ref[s, 0, h, rows, :] for s in chips], axis=0))
                 vs.append(jnp.concatenate([in_ref[s, 1, h, rows, :] for s in chips], axis=0))
-                q = jnp.concatenate([in_ref[s, 2, h, rows, :] for s in chips], axis=0)
+                q = jnp.concatenate([q_ref[s, h, rows, :] for s in chips], axis=0)
                 result, logs = attend(q, ks[b], ks[b + 1], vs[b], vs[b + 1], bias if b == 0 else None)
                 for i, s in enumerate(chips):
                     res_ref[s, h, rows, :] = result[i * 64 : (i + 1) * 64].astype(bf16)
@@ -268,23 +271,24 @@
         out[...] = res_ref[lax.rem(x + steps, ROW)]
 
 
-def row_attention(place, pieces, halo):
+def row_attention(place, pieces, asking, halo):
     shape = (ROW_HEADS, ROW_RETURN, HEAD)
     vmem = pl.BlockSpec(memory_space=pltpu.VMEM)
     return pl.pallas_call(
         row_kernel,
-        in_specs=[pl.BlockSpec(memory_space=pltpu.SMEM)] + [vmem] * (ROW + 1),
+        in_specs=[pl.BlockSpec(memory_space=pltpu.SMEM)] + [vmem] * (2 * ROW + 1),
         out_specs=[vmem] * ROW,
         out_shape=[jax.ShapeDtypeStruct(shape, bf16)] * ROW,
         scratch_shapes=[
-            pltpu.VMEM((ROW, 3, ROW_HEADS, TOKENS, HEAD), bf16),
+            pltpu.VMEM((ROW, 2, ROW_HEADS, TOKENS, HEAD), bf16),
+            pltpu.VMEM((ROW, ROW_HEADS, TOKENS, HEAD), bf16),
             pltpu.VMEM((ROW, *shape), bf16),
             pltpu.VMEM((ROW, ROW_HEADS, TOKENS, 1), f32),
         ],
         compiler_params=pltpu.CompilerParams(vmem_limit_bytes=12 * 2**20),
         cost_estimate=pl.CostEstimate(flops=2**31, bytes_accessed=3 * 2**20, transcendentals=2**19),
         name="row_attention",
-    )(place, *pieces, halo)
+    )(place, *pieces, *asking, halo)
 
 
 def near_kernel(
@@ -429,19 +433,22 @@
     start = device * TOKENS
     cosine, sine = tables(TOKENS, start)
 
-    edge = onward(jnp.stack([keys[0, HALF:], values[0, HALF:]]), 1)
     held = plane_pieces(keys, values, queries, cosine, sine)
     held = exchange(held)
-    own, *others = row_pieces(x, keys, values, queries, cosine, sine)
-    pieces = [own] + [along_row(block, steps) for steps, block in enumerate(others, 1)]
+    pieces, asking = row_pieces(x, keys, values, queries, cosine, sine)
+    pieces = pieces[:1] + [along_row(block, steps) for steps, block in enumerate(pieces[1:], 1)]
+    asking = asking[:1] + [along_row(block, steps) for steps, block in enumerate(asking[1:], 1)]
+    edge = jnp.stack([keys[0, HALF:], values[0, HALF:]])
+    up = lax.ppermute(edge, "sp", [(i, i + ROW) for i in range(ROW - 1, devices - ROW, ROW)])
     halo2 = onward(held[PLANE // 2 :, :2], PLANE)
+    edge = along_row(jnp.where(x[0] == ROW - 1, up, edge), 1)
     last = pick_last(x, pieces)
     halo1 = onward(last, ROW)
     pcos, psin = tables(HALF, start - HALF)
     near, log = near_attention(device.reshape(1), cosine, sine, pcos, psin, queries, keys, values, edge)
     far = plane_attention((device // PLANE).reshape(1), held, halo2)
     far = exchange(far)
-    mine, *sent = row_attention(jnp.stack([x[0], device // ROW]), pieces, halo1)
+    mine, *sent = row_attention(jnp.stack([x[0], device // ROW]), pieces, asking, halo1)
     back = [along_row(block, steps) for steps, block in enumerate(sent, 1)]
     attended = merge_groups(x, near, log, far, mine, back)
     other = lax.ppermute(attended, "tp", [(0, 1), (1, 0)])

time: 117 us -> 114 us (0.974)
  the two profiles are of different devices: /device:TPU:9 before, /device:TPU:65 now
where the time goes in v1:
time: 114 us; the launch traced here: 113 us
  starting transfers between devices  47.9 us (42%)
  waiting for transfers between devices  28.1 us (25%)
  Pallas kernels  24.7 us (22%)
  local copies, waits for them, and re-layouts  7.87 us (7%)
  other arithmetic  4.04 us (4%)
    all_to_all x1, waiting for transfers between devices, shards(): held = exchange(held)  19.8 us
    ppermute x10, starting transfers between devices, along_row(): lax.ppermute(block, 'sp', [(i, i // ROW * ROW + (i + steps) % ROW) for i...  11 us
    ppermute x1, starting transfers between devices, shards(): other = lax.ppermute(attended, 'tp', [(0, 1), (1, 0)])  10.5 us
    all_to_all x1, starting transfers between devices, shards(): far = exchange(far)  9.66 us
    ppermute x2, starting transfers between devices, onward(): lax.ppermute(block, 'sp', [(i, i + distance) for i in range(devices - dis...  8.51 us
    ppermute x10, waiting for transfers between devices, along_row(): lax.ppermute(block, 'sp', [(i, i // ROW * ROW + (i + steps) % ROW) for i...  6.78 us
    all_to_all x1, starting transfers between devices, shards(): held = exchange(held)  6.77 us
    pallas_call x1, Pallas kernels, near_attention(): pl.pallas_call(near_kernel, in_specs=[pl.BlockSpec(memory_space=pltpu.SME...  5.68 us
  transfers between devices with their start and end apart: 16, of which 4 were waited for; matrix products, arithmetic and copies ran while one was open for 5% of the time, Pallas kernels for 15%

profile of v1, /device:TPU:65, one launch (start us, length us, event | category | flops | bytes accessed | tf_op | source)
XLA Modules:
  0.0 112.9 jit_solution(17114813845116349898)
XLA Ops:
  0.0 1.2 %multiply_sine_fusion = (f32[256,64]{1,0:T(8,128)}, f32[256,64]{1,0:T(8,128)}) fusion(f32[64]{0:T(128)S(1)} %multiply_power_fusion, f32[256]{0:T(256)S(1)} %add_convert_fusion), kind=kLoop, calls=%fused_computation.2 | loop fusion | flops 16384 | bytes 132352 | tf_op jit(solution)/shard_map/sin | solution.py:413
  1.3 4.5 %plane_pieces.1 = bf16[16,3,128,128]{3,2,1,0:T(8,128)(2,1)} custom-call(f32[256,64]{1,0:T(8,128)} %get-tuple-element.34.cos_ref, f32[256,64]{1,0:T(8,128)} %get-tuple-element.33.sin_ref, bf16[3,256,1024]{2,1,0:T(8,128)(2,1)} %k_ref.3, bf16[3,256,1024]{2,1,0:T(8,128)(2,1)} %v_ref.3, bf16[3,256,1024]{2,1,0:T(8,128)(2,1)} %q_ref.3), custom_call_target="tpu_custom_call" | custom-call | flops 1073741824 | bytes 3145728 | tf_op jit(solution)/shard_map/plane_pieces/pallas_call | solution.py:78
  5.8 6.8 %all-to-all-start = ((bf16[16,3,128,128]{3,2,1,0:T(8,128)(2,1)}), bf16[16,3,128,128]{3,2,1,0:T(8,128)(2,1)S(1)}, u32[]{:S(2)}, u32[]{:S(2)}) async-start(bf16[16,3,128,128]{3,2,1,0:T(8,128)(2,1)} %plane_pieces.1), calls=%async_computation | async-start | bytes 3145728 | tf_op jit(solution)/shard_map/all_to_all | solution.py:437
  12.5 1.0 slice.10
  13.5 1.0 slice.9
  14.5 0.0 copy-start.6
  14.5 0.9 pad_maximum_fusion
  15.4 1.5 %collective-permute-start = (bf16[2,128,1024]{2,1,0:T(8,128)(2,1)}, bf16[2,128,1024]{2,1,0:T(8,128)(2,1)}, u32[]{:S(2)}, u32[]{:S(2)}) collective-permute-start(bf16[2,128,1024]{2,1,0:T(8,128)(2,1)} %pad_maximum_fusion), channel_id=1, source_target_pairs={{6,14},{14,22},{22,30},{30,38},{38,46},{46,54},{54,62},{62,70},{70... | collective-permute-start | bytes 1572872 | tf_op jit(solution)/shard_map/ppermute | solution.py:442
  16.8 19.8 %all-to-all-done.in_ref = bf16[16,3,128,128]{3,2,1,0:T(8,128)(2,1)S(1)} async-done(((bf16[16,3,128,128]{3,2,1,0:T(8,128)(2,1)}), bf16[16,3,128,128]{3,2,1,0:T(8,128)(2,1)S(1)}, u32[]{:S(2)}, u32[]{:S(2)}) %all-to-all-start) | async-done | bytes 1572896 | tf_op jit(solution)/shard_map/all_to_all | solution.py:437
  36.6 0.8 slice.12
  37.5 3.5 %collective-permute-start.2 = (bf16[8,2,128,128]{3,2,1,0:T(8,128)(2,1)}, bf16[8,2,128,128]{3,2,1,0:T(8,128)(2,1)}, u32[]{:S(2)}, u32[]{:S(2)}) collective-permute-start(bf16[8,2,128,128]{3,2,1,0:T(8,128)(2,1)} %slice.12), channel_id=1, source_target_pairs={{0,32},{2,34},{4,36},{6,38},{8,40},{10,42},{12,44},{14,46},{16,48}... | collective-permute-start | bytes 1572872 | tf_op jit(solution)/shard_map/ppermute | solution.py:428
  41.0 3.8 %row_pieces.1 = (bf16[2,2,256,128]{3,2,1,0:T(8,128)(2,1)}, bf16[2,2,256,128]{3,2,1,0:T(8,128)(2,1)}, bf16[2,2,256,128]{3,2,1,0:T(8,128)(2,1)}, bf16[2,2,256,128]...) custom-call(s32[1]{0:T(128)} %bitcast.1.x_ref, ...), custom_call_target="tpu_custom_call" | custom-call | flops 1073741824 | bytes 3145728 | tf_op jit(solution)/shard_map/row_pieces/pallas_call | solution.py:124
  44.8 0.0 copy-done.6
  44.8 0.1 collective-permute-start.3
  44.9 3.3 %collective-permute-start.4 = (bf16[2,2,256,128]{3,2,1,0:T(8,128)(2,1)}, bf16[2,2,256,128]{3,2,1,0:T(8,128)(2,1)S(1)}, u32[]{:S(2)}, u32[]{:S(2)}) collective-permute-start(bf16[2,2,256,128]{3,2,1,0:T(8,128)(2,1)} %get-tuple-element.23), channel_id=1, source_target_pairs={{0,4},{2,6},{4,0},{6,2},{8,12},{10,14},{12,8},{14,10},{16,20},{18,... | collective-permute-start | bytes 786440 | tf_op jit(solution)/shard_map/ppermute | solution.py:425
  48.1 0.0 collective-permute-start.5
  48.2 3.3 %collective-permute-done.3.one_ref.refs_1_ = bf16[2,2,256,128]{3,2,1,0:T(8,128)(2,1)S(1)} collective-permute-done((bf16[2,2,256,128]{3,2,1,0:T(8,128)(2,1)}, bf16[2,2,256,128]{3,2,1,0:T(8,128)(2,1)S(1)}, u32[]{:S(2)}, u32[]{:S(2)}) %collective-permute-start.3) | collective-permute-done | bytes 262176 | tf_op jit(solution)/shard_map/ppermute | solution.py:425
  51.5 0.0 collective-permute-start.6
  51.5 3.4 %collective-permute-done.4.two_ref.refs_2_ = bf16[2,2,256,128]{3,2,1,0:T(8,128)(2,1)S(1)} collective-permute-done((bf16[2,2,256,128]{3,2,1,0:T(8,128)(2,1)}, bf16[2,2,256,128]{3,2,1,0:T(8,128)(2,1)S(1)}, u32[]{:S(2)}, u32[]{:S(2)}) %collective-permute-start.4) | collective-permute-done | bytes 262176 | tf_op jit(solution)/shard_map/ppermute | solution.py:425
  54.9 2.6 %collective-permute-start.7 = (bf16[2,256,128]{2,1,0:T(8,128)(2,1)}, bf16[2,256,128]{2,1,0:T(8,128)(2,1)S(1)}, u32[]{:S(2)}, u32[]{:S(2)}) collective-permute-start(bf16[2,256,128]{2,1,0:T(8,128)(2,1)} %get-tuple-element.27), channel_id=1, source_target_pairs={{0,4},{2,6},{4,0},{6,2},{8,12},{10,14},{12,8},{14,10},{16,20},{18,... | collective-permute-start | bytes 393224 | tf_op jit(solution)/shard_map/ppermute | solution.py:425
  57.5 0.0 collective-permute-done.5.three_ref.refs_3_
  57.5 0.0 collective-permute-start.8
  57.5 0.0 copy-start.2
  57.5 0.9 copy-done.2
  58.5 0.0 copy-start.7
  58.5 0.0 collective-permute-done
  58.5 5.0 %collective-permute-start.9 = (bf16[2,2,2,256,128]{4,3,2,1,0:T(8,128)(2,1)S(1)}, bf16[2,2,2,256,128]{4,3,2,1,0:T(8,128)(2,1)}, u32[]{:S(2)}, u32[]{:S(2)}) collective-permute-start(bf16[2,2,2,256,128]{4,3,2,1,0:T(8,128)(2,1)S(1)} %pick_last.1), channel_id=1, source_target_pairs={{0,8},{2,10},{4,12},{6,14},{8,16},{10,18},{12,20},{14,22},{16,24},... | collective-permute-start | bytes 1572872 | tf_op jit(solution)/shard_map/ppermute | solution.py:428
  63.5 0.0 copy-done.7
  63.5 0.9 broadcast_select_fusion
  64.4 0.0 collective-permute-done.2.halo_ref
  64.4 0.0 collective-permute-start.1
  64.4 0.0 copy-start.3
  64.4 0.0 copy-start.5
  64.4 3.6 %plane_attention.1 = bf16[16,144,128]{2,1,0:T(8,128)(2,1)} custom-call(s32[1]{0:T(128)} %bitcast.3.z_ref, bf16[16,3,128,128]{3,2,1,0:T(8,128)(2,1)S(1)} %all-to-all-done.in_ref, bf16[8,2,128,128]{3,2,1,0:T(8,128)(2,1)} %collective-permute-done.2.halo_ref), custom_call_target="tpu_custom_call" | custom-call | flops 2147483648 | bytes 3145728 | tf_op jit(solution)/shard_map/plane_attention/pallas_call | solution.py:207
  68.0 9.7 %all-to-all-start.1 = ((bf16[16,144,128]{2,1,0:T(8,128)(2,1)}), bf16[16,144,128]{2,1,0:T(8,128)(2,1)S(1)}, u32[]{:S(2)}, u32[]{:S(2)}) async-start(bf16[16,144,128]{2,1,0:T(8,128)(2,1)} %plane_attention.1), calls=%async_computation.1 | async-start | bytes 1179648 | tf_op jit(solution)/shard_map/all_to_all | solution.py:450
  77.7 1.0 multiply_sine_fusion.1
  78.7 0.1 pad_add_fusion.x_ref
  78.7 0.0 collective-permute-done.6.refs_5_
  78.7 0.0 collective-permute-done.7.refs_6_
  78.7 0.0 collective-permute-done.8.refs_7_
  78.7 0.0 collective-permute-done.9.refs_8_
  78.8 0.0 copy-done.3
  78.8 0.0 copy-done.5
  78.8 3.3 %row_attention.1 = (bf16[2,272,128]{2,1,0:T(8,128)(2,1)S(1)}, bf16[2,272,128]{2,1,0:T(8,128)(2,1)S(1)}, bf16[2,272,128]{2,1,0:T(8,128)(2,1)S(1)}, bf16[2,272,128]{2,1,0:T(8,128)(2,1)S(1)}) custom-call(s32[2]{0:T(128)S(1)} %pad_add_fusion.x_ref, bf16[2,2,256,128]{3,2,1,0:T(8,128)(2,1)S(1)} %copy-done.3, ...), custom_call_target="tpu_custom_call" | custom-call | flops 2147483648 | bytes 3145728 | tf_op jit(solution)/shard_map/row_attention/pallas_call | solution.py:277
  82.1 1.4 %collective-permute-start.10 = (bf16[2,272,128]{2,1,0:T(8,128)(2,1)S(1)}, bf16[2,272,128]{2,1,0:T(8,128)(2,1)S(1)}, u32[]{:S(2)}, u32[]{:S(2)}) collective-permute-start(bf16[2,272,128]{2,1,0:T(8,128)(2,1)S(1)} %get-tuple-element.30), channel_id=1, source_target_pairs={{0,2},{2,4},{4,6},{6,0},{8,10},{10,12},{12,14},{14,8},{16,18},{18,... | collective-permute-start | bytes 417800 | tf_op jit(solution)/shard_map/ppermute | solution.py:425
  83.6 2.4 %collective-permute-start.11 = (bf16[2,272,128]{2,1,0:T(8,128)(2,1)S(1)}, bf16[2,272,128]{2,1,0:T(8,128)(2,1)S(1)}, u32[]{:S(2)}, u32[]{:S(2)}) collective-permute-start(bf16[2,272,128]{2,1,0:T(8,128)(2,1)S(1)} %get-tuple-element.31), channel_id=1, source_target_pairs={{0,4},{2,6},{4,0},{6,2},{8,12},{10,14},{12,8},{14,10},{16,20},{18,... | collective-permute-start | bytes 417800 | tf_op jit(solution)/shard_map/ppermute | solution.py:425
  86.0 1.2 %collective-permute-start.12 = (bf16[2,272,128]{2,1,0:T(8,128)(2,1)S(1)}, bf16[2,272,128]{2,1,0:T(8,128)(2,1)S(1)}, u32[]{:S(2)}, u32[]{:S(2)}) collective-permute-start(bf16[2,272,128]{2,1,0:T(8,128)(2,1)S(1)} %get-tuple-element.32), channel_id=1, source_target_pairs={{0,6},{2,0},{4,2},{6,4},{8,14},{10,8},{12,10},{14,12},{16,22},{18,... | collective-permute-start | bytes 417800 | tf_op jit(solution)/shard_map/ppermute | solution.py:425
  87.2 0.0 collective-permute-done.1.halo_ref
  87.2 5.7 %near_attention.1 = (bf16[256,1024]{1,0:T(8,128)(2,1)}, f32[256,128]{1,0:T(8,128)}) custom-call(s32[1]{0:T(128)} %bitcast.2.z_ref, f32[256,64]{1,0:T(8,128)} %get-tuple-element.34.cos_ref, f32[256,64]{1,0:T(8,128)} %get-tuple-element.33.sin_ref, f32[128,64]{1,0:T(8,128)} %get-tuple-element.36.pcos_ref, f32[128,64]{1,0:T(8,128)} %get-tuple-element.35.psin_ref, ...), custom_call_target="tpu_custom_call" | custom-call | flops 2147483648 | bytes 4194304 | tf_op jit(solution)/shard_map/near_attention/pallas_call | solution.py:329
  92.9 0.0 collective-permute-done.10.one_ref
  92.9 0.0 collective-permute-done.11.two_ref
  92.9 0.0 collective-permute-done.12.three_ref
  92.9 0.0 all-to-all-done.1.far_ref
  92.9 0.0 copy-start.1
  92.9 1.0 copy-done.1
  93.9 0.0 copy-start.4
  93.9 0.9 copy-done.4
  94.8 1.8 %merge_groups.1.mine_ref = bf16[256,1024]{1,0:T(8,128)(2,1)S(1)} custom-call(s32[1]{0:T(128)} %bitcast.1.x_ref, bf16[256,1024]{1,0:T(8,128)(2,1)S(1)} %copy-done.1, f32[256,128]{1,0:T(8,128)S(1)} %copy-done.4, bf16[16,144,128]{2,1,0:T(8,128)(2,1)S(1)} %all-to-all-done.1.far_ref, bf16[2,272,128]{2,1,0:T(8,128)(2,1)S(1)} %get-tuple-element.29.own_ref, ...), custom_call_target="tpu_custom_call" | custom-call | flops 16777216 | bytes 2097152 | tf_op jit(solution)/shard_map/merge_groups/pallas_call | solution.py:375
  96.6 10.5 %collective-permute-start.13 = (bf16[256,1024]{1,0:T(8,128)(2,1)S(1)}, bf16[256,1024]{1,0:T(8,128)(2,1)S(1)}, u32[]{:S(2)}, u32[]{:S(2)}) collective-permute-start(bf16[256,1024]{1,0:T(8,128)(2,1)S(1)} %merge_groups.1.mine_ref), channel_id=1, source_target_pairs={{0,1},{1,0},{2,3},{3,2},{4,5},{5,4},{6,7},{7,6},{8,9},{9,8},{10,11... | collective-permute-start | bytes 1572872 | tf_op jit(solution)/shard_map/ppermute | solution.py:454
  107.1 1.5 %collective-permute-done.13.other_ref = bf16[256,1024]{1,0:T(8,128)(2,1)S(1)} collective-permute-done((bf16[256,1024]{1,0:T(8,128)(2,1)S(1)}, bf16[256,1024]{1,0:T(8,128)(2,1)S(1)}, u32[]{:S(2)}, u32[]{:S(2)}) %collective-permute-start.13) | collective-permute-done | bytes 524320 | tf_op jit(solution)/shard_map/ppermute | solution.py:454
  108.7 0.0 copy-start
  108.7 2.2 %copy-done = bf16[2048,1024]{1,0:T(8,128)(2,1)S(1)} copy-done((bf16[2048,1024]{1,0:T(8,128)(2,1)S(1)}, bf16[2048,1024]{1,0:T(8,128)(2,1)}, u32[]{:S(2)}) %copy-start) | copy-done | bytes 4194328
  110.9 2.0 %project.1 = bf16[256,1024]{1,0:T(8,128)(2,1)} custom-call(s32[1]{0:T(128)} %bitcast.core_ref, bf16[256,1024]{1,0:T(8,128)(2,1)S(1)} %merge_groups.1.mine_ref, bf16[256,1024]{1,0:T(8,128)(2,1)S(1)} %collective-permute-done.13.other_ref, bf16[2048,1024]{1,0:T(8,128)(2,1)S(1)} %copy-done), custom_call_target="tpu_custom_call" | custom-call | flops 1073741824 | bytes 4194304 | tf_op jit(solution)/shard_map/project/pallas_call | solution.py:399
  (4 shorter events, 0.1 us)
Async XLA Ops:
  5.8 30.9 %all-to-all-start = ((bf16[16,3,128,128]{3,2,1,0:T(8,128)(2,1)}), bf16[16,3,128,128]{3,2,1,0:T(8,128)(2,1)S(1)}, u32[]{:S(2)}, u32[]{:S(2)}) async-start(bf16[16,3,128,128]{3,2,1,0:T(8,128)(2,1)} %plane_pieces.1), calls=%async_computation | async-start | bytes 3145728 | tf_op jit(solution)/shard_map/all_to_all | solution.py:437
  14.5 30.3 %copy-start.6 = (bf16[1,128,1024]{2,1,0:T(8,128)(2,1)}, bf16[1,128,1024]{2,1,0:T(8,128)(2,1)S(1)}, u32[]{:S(2)}) copy-start(bf16[1,128,1024]{2,1,0:T(8,128)(2,1)S(1)} %slice.9) | copy-start | bytes 786436
  15.4 43.2 %collective-permute-start = (bf16[2,128,1024]{2,1,0:T(8,128)(2,1)}, bf16[2,128,1024]{2,1,0:T(8,128)(2,1)}, u32[]{:S(2)}, u32[]{:S(2)}) collective-permute-start(bf16[2,128,1024]{2,1,0:T(8,128)(2,1)} %pad_maximum_fusion), channel_id=1, source_target_pairs={{6,14},{14,22},{22,30},{30,38},{38,46},{46,54},{54,62},{62,70},{70... | collective-permute-start | bytes 1572872 | tf_op jit(solution)/shard_map/ppermute | solution.py:442
  37.5 27.0 %collective-permute-start.2 = (bf16[8,2,128,128]{3,2,1,0:T(8,128)(2,1)}, bf16[8,2,128,128]{3,2,1,0:T(8,128)(2,1)}, u32[]{:S(2)}, u32[]{:S(2)}) collective-permute-start(bf16[8,2,128,128]{3,2,1,0:T(8,128)(2,1)} %slice.12), channel_id=1, source_target_pairs={{0,32},{2,34},{4,36},{6,38},{8,40},{10,42},{12,44},{14,46},{16,48}... | collective-permute-start | bytes 1572872 | tf_op jit(solution)/shard_map/ppermute | solution.py:428
  44.8 6.7 %collective-permute-start.3 = (bf16[2,2,256,128]{3,2,1,0:T(8,128)(2,1)}, bf16[2,2,256,128]{3,2,1,0:T(8,128)(2,1)S(1)}, u32[]{:S(2)}, u32[]{:S(2)}) collective-permute-start(bf16[2,2,256,128]{3,2,1,0:T(8,128)(2,1)} %get-tuple-element.22), channel_id=1, source_target_pairs={{0,2},{2,4},{4,6},{6,0},{8,10},{10,12},{12,14},{14,8},{16,18},{18,... | collective-permute-start | bytes 786440 | tf_op jit(solution)/shard_map/ppermute | solution.py:425
  44.9 10.1 %collective-permute-start.4 = (bf16[2,2,256,128]{3,2,1,0:T(8,128)(2,1)}, bf16[2,2,256,128]{3,2,1,0:T(8,128)(2,1)S(1)}, u32[]{:S(2)}, u32[]{:S(2)}) collective-permute-start(bf16[2,2,256,128]{3,2,1,0:T(8,128)(2,1)} %get-tuple-element.23), channel_id=1, source_target_pairs={{0,4},{2,6},{4,0},{6,2},{8,12},{10,14},{12,8},{14,10},{16,20},{18,... | collective-permute-start | bytes 786440 | tf_op jit(solution)/shard_map/ppermute | solution.py:425
  48.1 9.4 %collective-permute-start.5 = (bf16[2,2,256,128]{3,2,1,0:T(8,128)(2,1)}, bf16[2,2,256,128]{3,2,1,0:T(8,128)(2,1)S(1)}, u32[]{:S(2)}, u32[]{:S(2)}) collective-permute-start(bf16[2,2,256,128]{3,2,1,0:T(8,128)(2,1)} %get-tuple-element.24), channel_id=1, source_target_pairs={{0,6},{2,0},{4,2},{6,4},{8,14},{10,8},{12,10},{14,12},{16,22},{18,... | collective-permute-start | bytes 786440 | tf_op jit(solution)/shard_map/ppermute | solution.py:425
  51.5 27.2 %collective-permute-start.6 = (bf16[2,256,128]{2,1,0:T(8,128)(2,1)}, bf16[2,256,128]{2,1,0:T(8,128)(2,1)S(1)}, u32[]{:S(2)}, u32[]{:S(2)}) collective-permute-start(bf16[2,256,128]{2,1,0:T(8,128)(2,1)} %get-tuple-element.26), channel_id=1, source_target_pairs={{0,2},{2,4},{4,6},{6,0},{8,10},{10,12},{12,14},{14,8},{16,18},{18,... | collective-permute-start | bytes 393224 | tf_op jit(solution)/shard_map/ppermute | solution.py:425
  54.9 23.8 %collective-permute-start.7 = (bf16[2,256,128]{2,1,0:T(8,128)(2,1)}, bf16[2,256,128]{2,1,0:T(8,128)(2,1)S(1)}, u32[]{:S(2)}, u32[]{:S(2)}) collective-permute-start(bf16[2,256,128]{2,1,0:T(8,128)(2,1)} %get-tuple-element.27), channel_id=1, source_target_pairs={{0,4},{2,6},{4,0},{6,2},{8,12},{10,14},{12,8},{14,10},{16,20},{18,... | collective-permute-start | bytes 393224 | tf_op jit(solution)/shard_map/ppermute | solution.py:425
  57.5 21.2 %collective-permute-start.8 = (bf16[2,256,128]{2,1,0:T(8,128)(2,1)}, bf16[2,256,128]{2,1,0:T(8,128)(2,1)}, u32[]{:S(2)}, u32[]{:S(2)}) collective-permute-start(bf16[2,256,128]{2,1,0:T(8,128)(2,1)} %get-tuple-element.28), channel_id=1, source_target_pairs={{0,6},{2,0},{4,2},{6,4},{8,14},{10,8},{12,10},{14,12},{16,22},{18,... | collective-permute-start | bytes 393224 | tf_op jit(solution)/shard_map/ppermute | solution.py:425
  57.5 1.0 copy-start.2
  58.5 5.0 %copy-start.7 = (bf16[1,128,1024]{2,1,0:T(8,128)(2,1)S(1)}, bf16[1,128,1024]{2,1,0:T(8,128)(2,1)}, u32[]{:S(2)}) copy-start(bf16[1,128,1024]{2,1,0:T(8,128)(2,1)} %copy-done.6) | copy-start | bytes 786436
  58.5 20.2 %collective-permute-start.9 = (bf16[2,2,2,256,128]{4,3,2,1,0:T(8,128)(2,1)S(1)}, bf16[2,2,2,256,128]{4,3,2,1,0:T(8,128)(2,1)}, u32[]{:S(2)}, u32[]{:S(2)}) collective-permute-start(bf16[2,2,2,256,128]{4,3,2,1,0:T(8,128)(2,1)S(1)} %pick_last.1), channel_id=1, source_target_pairs={{0,8},{2,10},{4,12},{6,14},{8,16},{10,18},{12,20},{14,22},{16,24},... | collective-permute-start | bytes 1572872 | tf_op jit(solution)/shard_map/ppermute | solution.py:428
  64.4 22.8 %collective-permute-start.1 = (bf16[2,128,1024]{2,1,0:T(8,128)(2,1)}, bf16[2,128,1024]{2,1,0:T(8,128)(2,1)}, u32[]{:S(2)}, u32[]{:S(2)}) collective-permute-start(bf16[2,128,1024]{2,1,0:T(8,128)(2,1)} %broadcast_select_fusion), channel_id=1, source_target_pairs={{0,2},{2,4},{4,6},{6,0},{8,10},{10,12},{12,14},{14,8},{16,18},{18,... | collective-permute-start | bytes 1572872 | tf_op jit(solution)/shard_map/ppermute | solution.py:425
  64.4 14.3 %copy-start.3 = (bf16[2,2,256,128]{3,2,1,0:T(8,128)(2,1)S(1)}, bf16[2,2,256,128]{3,2,1,0:T(8,128)(2,1)}, u32[]{:S(2)}) copy-start(bf16[2,2,256,128]{3,2,1,0:T(8,128)(2,1)} %get-tuple-element.21.own_ref.refs_0_) | copy-start | bytes 786436
  64.4 14.3 %copy-start.5 = (bf16[2,256,128]{2,1,0:T(8,128)(2,1)S(1)}, bf16[2,256,128]{2,1,0:T(8,128)(2,1)}, u32[]{:S(2)}) copy-start(bf16[2,256,128]{2,1,0:T(8,128)(2,1)} %get-tuple-element.25.refs_4_) | copy-start | bytes 393220
  68.0 24.9 %all-to-all-start.1 = ((bf16[16,144,128]{2,1,0:T(8,128)(2,1)}), bf16[16,144,128]{2,1,0:T(8,128)(2,1)S(1)}, u32[]{:S(2)}, u32[]{:S(2)}) async-start(bf16[16,144,128]{2,1,0:T(8,128)(2,1)} %plane_attention.1), calls=%async_computation.1 | async-start | bytes 1179648 | tf_op jit(solution)/shard_map/all_to_all | solution.py:450
  82.1 10.7 %collective-permute-start.10 = (bf16[2,272,128]{2,1,0:T(8,128)(2,1)S(1)}, bf16[2,272,128]{2,1,0:T(8,128)(2,1)S(1)}, u32[]{:S(2)}, u32[]{:S(2)}) collective-permute-start(bf16[2,272,128]{2,1,0:T(8,128)(2,1)S(1)} %get-tuple-element.30), channel_id=1, source_target_pairs={{0,2},{2,4},{4,6},{6,0},{8,10},{10,12},{12,14},{14,8},{16,18},{18,... | collective-permute-start | bytes 417800 | tf_op jit(solution)/shard_map/ppermute | solution.py:425
  83.6 9.3 %collective-permute-start.11 = (bf16[2,272,128]{2,1,0:T(8,128)(2,1)S(1)}, bf16[2,272,128]{2,1,0:T(8,128)(2,1)S(1)}, u32[]{:S(2)}, u32[]{:S(2)}) collective-permute-start(bf16[2,272,128]{2,1,0:T(8,128)(2,1)S(1)} %get-tuple-element.31), channel_id=1, source_target_pairs={{0,4},{2,6},{4,0},{6,2},{8,12},{10,14},{12,8},{14,10},{16,20},{18,... | collective-permute-start | bytes 417800 | tf_op jit(solution)/shard_map/ppermute | solution.py:425
  86.0 6.9 %collective-permute-start.12 = (bf16[2,272,128]{2,1,0:T(8,128)(2,1)S(1)}, bf16[2,272,128]{2,1,0:T(8,128)(2,1)S(1)}, u32[]{:S(2)}, u32[]{:S(2)}) collective-permute-start(bf16[2,272,128]{2,1,0:T(8,128)(2,1)S(1)} %get-tuple-element.32), channel_id=1, source_target_pairs={{0,6},{2,0},{4,2},{6,4},{8,14},{10,8},{12,10},{14,12},{16,22},{18,... | collective-permute-start | bytes 417800 | tf_op jit(solution)/shard_map/ppermute | solution.py:425
  92.9 1.0 copy-start.1
  93.9 0.9 copy-start.4
  96.6 12.0 %collective-permute-start.13 = (bf16[256,1024]{1,0:T(8,128)(2,1)S(1)}, bf16[256,1024]{1,0:T(8,128)(2,1)S(1)}, u32[]{:S(2)}, u32[]{:S(2)}) collective-permute-start(bf16[256,1024]{1,0:T(8,128)(2,1)S(1)} %merge_groups.1.mine_ref), channel_id=1, source_target_pairs={{0,1},{1,0},{2,3},{3,2},{4,5},{5,4},{6,7},{7,6},{8,9},{9,8},{10,11... | collective-permute-start | bytes 1572872 | tf_op jit(solution)/shard_map/ppermute | solution.py:454
  108.7 2.2 %copy-start = (bf16[2048,1024]{1,0:T(8,128)(2,1)S(1)}, bf16[2048,1024]{1,0:T(8,128)(2,1)}, u32[]{:S(2)}) copy-start(bf16[2048,1024]{1,0:T(8,128)(2,1)} %w_ref.1) | copy-start | bytes 12582916

commit v2 on v1

--- a/solution.py
+++ b/solution.py
@@ -291,56 +291,60 @@
     )(place, *pieces, *asking, halo)
 
 
-def near_kernel(
-    z_ref, cos_ref, sin_ref, pcos_ref, psin_ref, q_hbm, k_hbm, v_hbm, halo_ref, out_ref, log_ref, q_ref, k_ref, v_ref, sem
-):
-    pairs = ((q_hbm, q_ref), (k_hbm, k_ref), (v_hbm, v_ref))
-    copies = [pltpu.make_async_copy(a.at[0], b, sem.at[i]) for i, (a, b) in enumerate(pairs)]
+def near_kernel(half, z_ref, cos_ref, sin_ref, pcos_ref, psin_ref, q_hbm, k_hbm, v_hbm, *refs):
+    halo_ref, (out_ref, q_ref, k_ref, v_ref, sem) = refs[0], refs[-5:]
+    rows = pl.ds(half * HALF, HALF)
+    span = pl.ds(0, (half + 1) * HALF)
+    pairs = ((q_hbm.at[0, rows], q_ref), (k_hbm.at[0, span], k_ref), (v_hbm.at[0, span], v_ref))
+    copies = [pltpu.make_async_copy(a, b, sem.at[i]) for i, (a, b) in enumerate(pairs)]
     for copy in copies:
         copy.start()
-    bias = jnp.where(z_ref[0] == 0, MASKED, -MASKED)
     cosine, sine = full_tables(cos_ref, sin_ref)
     pcos, psin = full_tables(pcos_ref, psin_ref)
-    lane = iota((TOKENS, HEAD), 1)
-
-    held = jnp.zeros((TOKENS, HEAD), f32)
+    bias = jnp.where(z_ref[0] == 0, MASKED, -MASKED) if half == 0 else None
+    lane = iota((HALF, HEAD), 1)
+    held = jnp.zeros((HALF, HEAD), f32)
+    mine = slice(half * HALF, (half + 1) * HALF)
     for copy in copies:
         copy.wait()
     for h in range(LOCAL):
         lanes = slice(h * HEAD, (h + 1) * HEAD)
-        q = (turned(q_ref[:, lanes], cosine, sine) * SCALE).astype(bf16)
-        k = turned(k_ref[:, lanes], cosine, sine).astype(bf16)
+        q = (turned(q_ref[:, lanes], cosine[mine], sine[mine]) * SCALE).astype(bf16)
+        k = turned(k_ref[:, lanes], cosine[: (half + 1) * HALF], sine[: (half + 1) * HALF]).astype(bf16)
         v = v_ref[:, lanes]
-        ks = [turned(halo_ref[0, :, lanes], pcos, psin).astype(bf16), k[:HALF], k[HALF:]]
-        vs = [halo_ref[1, :, lanes], v[:HALF], v[HALF:]]
-        parts = []
-        for b in range(2):
-            result, logs = attend(
-                q[b * HALF : (b + 1) * HALF], ks[b], ks[b + 1], vs[b], vs[b + 1], bias if b == 0 else None
-            )
-            out_ref[b * HALF : (b + 1) * HALF, lanes] = result.astype(bf16)
-            parts.append(wide(logs))
-        held = jnp.where(lane == h, jnp.concatenate(parts, axis=0), held)
-    log_ref[...] = held
-
-
-def near_attention(device, cosine, sine, pcos, psin, queries, keys, values, halo):
+        if half == 0:
+            k_prev, v_prev = turned(halo_ref[0, :, lanes], pcos, psin).astype(bf16), halo_ref[1, :, lanes]
+        else:
+            k_prev, v_prev, k, v = k[:HALF], v[:HALF], k[HALF:], v[HALF:]
+        result, logs = attend(q, k_prev, k, v_prev, v, bias)
+        out_ref[:, lanes] = result.astype(bf16)
+        held = jnp.where(lane == h, wide(logs), held)
+    high = held.astype(bf16)
+    out_ref[:, LOCAL * HEAD : (LOCAL + 1) * HEAD] = high
+    out_ref[:, (LOCAL + 1) * HEAD :] = (held - high.astype(f32)).astype(bf16)
+
+
+def near_attention(half, device, cosine, sine, pcos, psin, queries, keys, values, halo):
     vmem, hbm = pl.BlockSpec(memory_space=pltpu.VMEM), pl.BlockSpec(memory_space=pltpu.HBM)
-    return pl.pallas_call(
-        near_kernel,
-        in_specs=[pl.BlockSpec(memory_space=pltpu.SMEM)] + [vmem] * 4 + [hbm] * 3 + [vmem],
-        out_specs=[vmem] * 2,
-        out_shape=[
-            jax.ShapeDtypeStruct((TOKENS, LOCAL * HEAD), bf16),
-            jax.ShapeDtypeStruct((TOKENS, HEAD), f32),
+    halo = [halo] if half == 0 else []
+    width = LOCAL * HEAD
+    return pl.pallas_call(
+        functools.partial(near_kernel, half),
+        in_specs=[pl.BlockSpec(memory_space=pltpu.SMEM)] + [vmem] * 4 + [hbm] * 3 + [vmem] * len(halo),
+        out_specs=vmem,
+        out_shape=jax.ShapeDtypeStruct((HALF, width + 2 * HEAD), bf16),
+        scratch_shapes=[
+            pltpu.VMEM((HALF, width), bf16),
+            pltpu.VMEM(((half + 1) * HALF, width), bf16),
+            pltpu.VMEM(((half + 1) * HALF, width), bf16),
+            pltpu.SemaphoreType.DMA((3,)),
         ],
-        scratch_shapes=[pltpu.VMEM((TOKENS, LOCAL * HEAD), bf16)] * 3 + [pltpu.SemaphoreType.DMA((3,))],
-        cost_estimate=pl.CostEstimate(flops=2**31, bytes_accessed=4 * 2**20, transcendentals=2**19),
+        cost_estimate=pl.CostEstimate(flops=2**30, bytes_accessed=2 * 2**20, transcendentals=2**18),
         name="near_attention",
-    )(device, cosine, sine, pcos, psin, queries, keys, values, halo)
-
-
-def merge_kernel(x_ref, near_ref, log_ref, far_ref, own_ref, one_ref, two_ref, three_ref, out_ref, far, far_log, mid, mid_log, row_ref):
+    )(device, cosine, sine, pcos, psin, queries, keys, values, *halo)
+
+
+def merge_kernel(x_ref, early_ref, late_ref, far_ref, own_ref, one_ref, two_ref, three_ref, out_ref, far, far_log, mid, mid_log, row_ref):
     x = x_ref[0]
     for steps, ref in enumerate((own_ref, one_ref, two_ref, three_ref)):
         row_ref[lax.rem(x + ROW - steps, ROW)] = ref[...]
@@ -362,14 +366,20 @@
                 target = pl.ds(r, 64, stride=4)
                 mid[h % 2, target, :] = row_ref[chip, head, r * 64 : (r + 1) * 64, :].astype(f32)
                 mid_log[h % 2, target, :] = logs[i * 64 : (i + 1) * 64]
-        logs = [wide(log_ref[:, h : h + 1]), mid_log[h % 2], far_log[h % 2]]
+        near, near_log = [], []
+        for ref in (late_ref, early_ref):
+            near.append(ref[:, lanes].astype(f32))
+            at = LOCAL * HEAD + h
+            near_log.append(wide(ref[:, at : at + 1].astype(f32) + ref[:, at + HEAD : at + HEAD + 1].astype(f32)))
+        near = jnp.concatenate(near, axis=0)
+        logs = [jnp.concatenate(near_log, axis=0), mid_log[h % 2], far_log[h % 2]]
         top = jnp.maximum(jnp.maximum(logs[0], logs[1]), logs[2])
         e = [jnp.exp(x - top) for x in logs]
-        total = e[0] * near_ref[:, lanes].astype(f32) + e[1] * mid[h % 2] + e[2] * far[h % 2]
+        total = e[0] * near + e[1] * mid[h % 2] + e[2] * far[h % 2]
         out_ref[:, lanes] = (total / (e[0] + e[1] + e[2])).astype(bf16)
 
 
-def merge_groups(x, near, log, far, own, others):
+def merge_groups(x, early, late, far, own, others):
 
     vmem = pl.BlockSpec(memory_space=pltpu.VMEM)
     return pl.pallas_call(
@@ -381,30 +391,30 @@
         compiler_params=pltpu.CompilerParams(vmem_limit_bytes=8 * 2**20),
         cost_estimate=pl.CostEstimate(flops=2**24, bytes_accessed=2**21, transcendentals=2**19),
         name="merge_groups",
-    )(x, near, log, far, own, *others)
-
-
-def project_kernel(core_ref, mine_ref, other_ref, w_ref, out_ref):
+    )(x, early, late, far, own, *others)
+
+
+def project_kernel(core_ref, in_ref, w_ref, *refs):
+    *partial, out_ref = refs
     half = LOCAL * HEAD
-    core = core_ref[0]
-    mine = pl.ds(pl.multiple_of(core * half, half), half)
-    other = pl.ds(pl.multiple_of((1 - core) * half, half), half)
-    total = jnp.dot(mine_ref[...], w_ref[mine, :], preferred_element_type=f32)
-    total += jnp.dot(other_ref[...], w_ref[other, :], preferred_element_type=f32)
-    out_ref[...] = total.astype(bf16)
-
-
-def project(core, mine, other, w_out):
+    rows = pl.ds(pl.multiple_of(core_ref[0] * half, half), half)
+    total = jnp.dot(in_ref[...], w_ref[rows, :], preferred_element_type=f32)
+    if partial:
+        total += partial[0][...]
+    out_ref[...] = total.astype(out_ref.dtype)
+
+
+def project(core, block, w_out, partial, dtype):
     vmem = pl.BlockSpec(memory_space=pltpu.VMEM)
     return pl.pallas_call(
         project_kernel,
-        in_specs=[pl.BlockSpec(memory_space=pltpu.SMEM), vmem, vmem, vmem],
+        in_specs=[pl.BlockSpec(memory_space=pltpu.SMEM)] + [vmem] * (2 + len(partial)),
         out_specs=vmem,
-        out_shape=jax.ShapeDtypeStruct((TOKENS, w_out.shape[1]), bf16),
+        out_shape=jax.ShapeDtypeStruct((TOKENS, w_out.shape[1]), dtype),
         compiler_params=pltpu.CompilerParams(vmem_limit_bytes=8 * 2**20),
-        cost_estimate=pl.CostEstimate(flops=2**30, bytes_accessed=2**22, transcendentals=0),
+        cost_estimate=pl.CostEstimate(flops=2**29, bytes_accessed=2**22, transcendentals=0),
         name="project",
-    )(core, mine, other, w_out)
+    )(core, block, w_out, *partial)
 
 
 def tables(count, start):
@@ -445,14 +455,17 @@
     last = pick_last(x, pieces)
     halo1 = onward(last, ROW)
     pcos, psin = tables(HALF, start - HALF)
-    near, log = near_attention(device.reshape(1), cosine, sine, pcos, psin, queries, keys, values, edge)
+    near_args = (device.reshape(1), cosine, sine, pcos, psin, queries, keys, values, edge)
+    early = near_attention(1, *near_args)
+    late = near_attention(0, *near_args)
     far = plane_attention((device // PLANE).reshape(1), held, halo2)
     far = exchange(far)
     mine, *sent = row_attention(jnp.stack([x[0], device // ROW]), pieces, asking, halo1)
     back = [along_row(block, steps) for steps, block in enumerate(sent, 1)]
-    attended = merge_groups(x, near, log, far, mine, back)
+    attended = merge_groups(x, early, late, far, mine, back)
     other = lax.ppermute(attended, "tp", [(0, 1), (1, 0)])
-    return project(core, attended, other, w_out)
+    partial = project(core, attended, w_out, (), f32)
+    return project(1 - core, other, w_out, (partial,), bf16)
 
 
 def solution(mesh):

time: 114 us -> 115 us (level)
  Pallas kernels: 24.7 us -> 27.5 us
  waiting for transfers between devices: 28.1 us -> 26.6 us
    pallas_call x1 -> x2, Pallas kernels: 5.68 us -> 8.25 us  [near_attention(): pl.pallas_call(functools.partial(near_kernel, half), in_specs=[pl.BlockSp...]
    ppermute x1, waiting for transfers between devices: 1.54 us -> 0.01 us  [shards(): other = lax.ppermute(attended, 'tp', [(0, 1), (1, 0)])]
    unnamed x16 -> x18, local copies, waits for them, and re-layouts: 5.09 us -> 5.59 us
  transfers between devices with their start and end apart: 16 -> 16, of which waited for: 4 -> 3; matrix products, arithmetic and copies ran while one was open for 5% -> 5% of each run, Pallas kernels for 15% -> 17%
where the time goes in v2:
time: 115 us
  starting transfers between devices  47.9 us (42%)
  Pallas kernels  27.5 us (24%)
  waiting for transfers between devices  26.6 us (23%)
  local copies, waits for them, and re-layouts  8.36 us (7%)
  other arithmetic  4.04 us (4%)
    all_to_all x1, waiting for transfers between devices, shards(): held = exchange(held)  19.8 us
    ppermute x10, starting transfers between devices, along_row(): lax.ppermute(block, 'sp', [(i, i // ROW * ROW + (i + steps) % ROW) for i...  11 us
    ppermute x1, starting transfers between devices, shards(): other = lax.ppermute(attended, 'tp', [(0, 1), (1, 0)])  10.5 us
    all_to_all x1, starting transfers between devices, shards(): far = exchange(far)  9.66 us
    ppermute x2, starting transfers between devices, onward(): lax.ppermute(block, 'sp', [(i, i + distance) for i in range(devices - dis...  8.51 us
    pallas_call x2, Pallas kernels, near_attention(): pl.pallas_call(functools.partial(near_kernel, half), in_specs=[pl.BlockSp...  8.25 us
    ppermute x10, waiting for transfers between devices, along_row(): lax.ppermute(block, 'sp', [(i, i // ROW * ROW + (i + steps) % ROW) for i...  6.78 us
    all_to_all x1, starting transfers between devices, shards(): held = exchange(held)  6.77 us
  transfers between devices with their start and end apart: 16, of which 3 were waited for; matrix products, arithmetic and copies ran while one was open for 5% of the time, Pallas kernels for 17%

profile of v2, /device:TPU:65, one launch (start us, length us, event | category | flops | bytes accessed | tf_op | source)
XLA Modules:
  0.0 114.7 jit_solution(9948437219870074969)
XLA Ops:
  0.0 1.2 %multiply_sine_fusion = (f32[256,64]{1,0:T(8,128)}, f32[256,64]{1,0:T(8,128)}) fusion(f32[64]{0:T(128)S(1)} %multiply_power_fusion, f32[256]{0:T(256)S(1)} %add_convert_fusion), kind=kLoop, calls=%fused_computation.2 | loop fusion | flops 16384 | bytes 132352 | tf_op jit(solution)/shard_map/sin | solution.py:423
  1.3 4.5 %plane_pieces.1 = bf16[16,3,128,128]{3,2,1,0:T(8,128)(2,1)} custom-call(f32[256,64]{1,0:T(8,128)} %get-tuple-element.30.cos_ref, f32[256,64]{1,0:T(8,128)} %get-tuple-element.29.sin_ref, bf16[3,256,1024]{2,1,0:T(8,128)(2,1)} %k_ref.3, bf16[3,256,1024]{2,1,0:T(8,128)(2,1)} %v_ref.3, bf16[3,256,1024]{2,1,0:T(8,128)(2,1)} %q_ref.3), custom_call_target="tpu_custom_call" | custom-call | flops 1073741824 | bytes 3145728 | tf_op jit(solution)/shard_map/plane_pieces/pallas_call | solution.py:78
  5.8 6.8 %all-to-all-start = ((bf16[16,3,128,128]{3,2,1,0:T(8,128)(2,1)}), bf16[16,3,128,128]{3,2,1,0:T(8,128)(2,1)S(1)}, u32[]{:S(2)}, u32[]{:S(2)}) async-start(bf16[16,3,128,128]{3,2,1,0:T(8,128)(2,1)} %plane_pieces.1), calls=%async_computation | async-start | bytes 3145728 | tf_op jit(solution)/shard_map/all_to_all | solution.py:447
  12.5 1.0 slice.10
  13.5 1.0 slice.9
  14.5 0.0 copy-start.7
  14.5 0.9 pad_maximum_fusion
  15.4 1.5 %collective-permute-start = (bf16[2,128,1024]{2,1,0:T(8,128)(2,1)}, bf16[2,128,1024]{2,1,0:T(8,128)(2,1)}, u32[]{:S(2)}, u32[]{:S(2)}) collective-permute-start(bf16[2,128,1024]{2,1,0:T(8,128)(2,1)} %pad_maximum_fusion), channel_id=1, source_target_pairs={{6,14},{14,22},{22,30},{30,38},{38,46},{46,54},{54,62},{62,70},{70... | collective-permute-start | bytes 1572872 | tf_op jit(solution)/shard_map/ppermute | solution.py:452
  16.8 19.8 %all-to-all-done.in_ref = bf16[16,3,128,128]{3,2,1,0:T(8,128)(2,1)S(1)} async-done(((bf16[16,3,128,128]{3,2,1,0:T(8,128)(2,1)}), bf16[16,3,128,128]{3,2,1,0:T(8,128)(2,1)S(1)}, u32[]{:S(2)}, u32[]{:S(2)}) %all-to-all-start) | async-done | bytes 1572896 | tf_op jit(solution)/shard_map/all_to_all | solution.py:447
  36.6 0.8 slice.12
  37.5 3.5 %collective-permute-start.2 = (bf16[8,2,128,128]{3,2,1,0:T(8,128)(2,1)}, bf16[8,2,128,128]{3,2,1,0:T(8,128)(2,1)}, u32[]{:S(2)}, u32[]{:S(2)}) collective-permute-start(bf16[8,2,128,128]{3,2,1,0:T(8,128)(2,1)} %slice.12), channel_id=1, source_target_pairs={{0,32},{2,34},{4,36},{6,38},{8,40},{10,42},{12,44},{14,46},{16,48}... | collective-permute-start | bytes 1572872 | tf_op jit(solution)/shard_map/ppermute | solution.py:438
  41.0 3.8 %row_pieces.1 = (bf16[2,2,256,128]{3,2,1,0:T(8,128)(2,1)}, bf16[2,2,256,128]{3,2,1,0:T(8,128)(2,1)}, bf16[2,2,256,128]{3,2,1,0:T(8,128)(2,1)}, bf16[2,2,256,128]...) custom-call(s32[1]{0:T(128)} %bitcast.1.x_ref, ...), custom_call_target="tpu_custom_call" | custom-call | flops 1073741824 | bytes 3145728 | tf_op jit(solution)/shard_map/row_pieces/pallas_call | solution.py:124
  44.8 0.0 copy-done.7
  44.8 0.1 collective-permute-start.3
  44.9 3.3 %collective-permute-start.4 = (bf16[2,2,256,128]{3,2,1,0:T(8,128)(2,1)}, bf16[2,2,256,128]{3,2,1,0:T(8,128)(2,1)S(1)}, u32[]{:S(2)}, u32[]{:S(2)}) collective-permute-start(bf16[2,2,256,128]{3,2,1,0:T(8,128)(2,1)} %get-tuple-element.19), channel_id=1, source_target_pairs={{0,4},{2,6},{4,0},{6,2},{8,12},{10,14},{12,8},{14,10},{16,20},{18,... | collective-permute-start | bytes 786440 | tf_op jit(solution)/shard_map/ppermute | solution.py:435
  48.1 0.0 collective-permute-start.5
  48.2 3.3 %collective-permute-done.3.one_ref.refs_1_ = bf16[2,2,256,128]{3,2,1,0:T(8,128)(2,1)S(1)} collective-permute-done((bf16[2,2,256,128]{3,2,1,0:T(8,128)(2,1)}, bf16[2,2,256,128]{3,2,1,0:T(8,128)(2,1)S(1)}, u32[]{:S(2)}, u32[]{:S(2)}) %collective-permute-start.3) | collective-permute-done | bytes 262176 | tf_op jit(solution)/shard_map/ppermute | solution.py:435
  51.5 0.0 collective-permute-start.6
  51.5 3.4 %collective-permute-done.4.two_ref.refs_2_ = bf16[2,2,256,128]{3,2,1,0:T(8,128)(2,1)S(1)} collective-permute-done((bf16[2,2,256,128]{3,2,1,0:T(8,128)(2,1)}, bf16[2,2,256,128]{3,2,1,0:T(8,128)(2,1)S(1)}, u32[]{:S(2)}, u32[]{:S(2)}) %collective-permute-start.4) | collective-permute-done | bytes 262176 | tf_op jit(solution)/shard_map/ppermute | solution.py:435
  54.9 2.6 %collective-permute-start.7 = (bf16[2,256,128]{2,1,0:T(8,128)(2,1)}, bf16[2,256,128]{2,1,0:T(8,128)(2,1)S(1)}, u32[]{:S(2)}, u32[]{:S(2)}) collective-permute-start(bf16[2,256,128]{2,1,0:T(8,128)(2,1)} %get-tuple-element.23), channel_id=1, source_target_pairs={{0,4},{2,6},{4,0},{6,2},{8,12},{10,14},{12,8},{14,10},{16,20},{18,... | collective-permute-start | bytes 393224 | tf_op jit(solution)/shard_map/ppermute | solution.py:435
  57.5 0.0 collective-permute-done.5.three_ref.refs_3_
  57.5 0.0 collective-permute-start.8
  57.5 0.0 copy-start.4
  57.5 0.9 copy-done.4
  58.5 0.0 copy-start.8
  58.5 0.0 collective-permute-done
  58.5 5.0 %collective-permute-start.9 = (bf16[2,2,2,256,128]{4,3,2,1,0:T(8,128)(2,1)S(1)}, bf16[2,2,2,256,128]{4,3,2,1,0:T(8,128)(2,1)}, u32[]{:S(2)}, u32[]{:S(2)}) collective-permute-start(bf16[2,2,2,256,128]{4,3,2,1,0:T(8,128)(2,1)S(1)} %pick_last.1), channel_id=1, source_target_pairs={{0,8},{2,10},{4,12},{6,14},{8,16},{10,18},{12,20},{14,22},{16,24},... | collective-permute-start | bytes 1572872 | tf_op jit(solution)/shard_map/ppermute | solution.py:438
  63.5 0.0 copy-done.8
  63.5 0.9 broadcast_select_fusion
  64.4 0.0 collective-permute-done.2.halo_ref
  64.4 0.0 collective-permute-start.1
  64.4 0.0 copy-start.6
  64.4 3.6 %plane_attention.1 = bf16[16,144,128]{2,1,0:T(8,128)(2,1)} custom-call(s32[1]{0:T(128)} %bitcast.3.z_ref, bf16[16,3,128,128]{3,2,1,0:T(8,128)(2,1)S(1)} %all-to-all-done.in_ref, bf16[8,2,128,128]{3,2,1,0:T(8,128)(2,1)} %collective-permute-done.2.halo_ref), custom_call_target="tpu_custom_call" | custom-call | flops 2147483648 | bytes 3145728 | tf_op jit(solution)/shard_map/plane_attention/pallas_call | solution.py:207
  68.0 9.7 %all-to-all-start.1 = ((bf16[16,144,128]{2,1,0:T(8,128)(2,1)}), bf16[16,144,128]{2,1,0:T(8,128)(2,1)S(1)}, u32[]{:S(2)}, u32[]{:S(2)}) async-start(bf16[16,144,128]{2,1,0:T(8,128)(2,1)} %plane_attention.1), calls=%async_computation.1 | async-start | bytes 1179648 | tf_op jit(solution)/shard_map/all_to_all | solution.py:462
  77.7 1.0 multiply_sine_fusion.1
  78.7 0.1 pad_add_fusion.x_ref
  78.7 0.0 collective-permute-done.6.refs_5_
  78.7 0.0 collective-permute-done.7.refs_6_
  78.7 0.0 collective-permute-done.8.refs_7_
  78.7 0.0 collective-permute-done.9.refs_8_
  78.8 0.0 copy-done.5
  78.8 0.0 copy-done.6
  78.8 3.3 %row_attention.1 = (bf16[2,272,128]{2,1,0:T(8,128)(2,1)S(1)}, bf16[2,272,128]{2,1,0:T(8,128)(2,1)S(1)}, bf16[2,272,128]{2,1,0:T(8,128)(2,1)S(1)}, bf16[2,272,128]{2,1,0:T(8,128)(2,1)S(1)}) custom-call(s32[2]{0:T(128)S(1)} %pad_add_fusion.x_ref, bf16[2,2,256,128]{3,2,1,0:T(8,128)(2,1)S(1)} %copy-done.5, ...), custom_call_target="tpu_custom_call" | custom-call | flops 2147483648 | bytes 3145728 | tf_op jit(solution)/shard_map/row_attention/pallas_call | solution.py:277
  82.1 1.4 %collective-permute-start.10 = (bf16[2,272,128]{2,1,0:T(8,128)(2,1)S(1)}, bf16[2,272,128]{2,1,0:T(8,128)(2,1)S(1)}, u32[]{:S(2)}, u32[]{:S(2)}) collective-permute-start(bf16[2,272,128]{2,1,0:T(8,128)(2,1)S(1)} %get-tuple-element.26), channel_id=1, source_target_pairs={{0,2},{2,4},{4,6},{6,0},{8,10},{10,12},{12,14},{14,8},{16,18},{18,... | collective-permute-start | bytes 417800 | tf_op jit(solution)/shard_map/ppermute | solution.py:435
  83.6 2.4 %collective-permute-start.11 = (bf16[2,272,128]{2,1,0:T(8,128)(2,1)S(1)}, bf16[2,272,128]{2,1,0:T(8,128)(2,1)S(1)}, u32[]{:S(2)}, u32[]{:S(2)}) collective-permute-start(bf16[2,272,128]{2,1,0:T(8,128)(2,1)S(1)} %get-tuple-element.27), channel_id=1, source_target_pairs={{0,4},{2,6},{4,0},{6,2},{8,12},{10,14},{12,8},{14,10},{16,20},{18,... | collective-permute-start | bytes 417800 | tf_op jit(solution)/shard_map/ppermute | solution.py:435
  86.0 1.2 %collective-permute-start.12 = (bf16[2,272,128]{2,1,0:T(8,128)(2,1)S(1)}, bf16[2,272,128]{2,1,0:T(8,128)(2,1)S(1)}, u32[]{:S(2)}, u32[]{:S(2)}) collective-permute-start(bf16[2,272,128]{2,1,0:T(8,128)(2,1)S(1)} %get-tuple-element.28), channel_id=1, source_target_pairs={{0,6},{2,0},{4,2},{6,4},{8,14},{10,8},{12,10},{14,12},{16,22},{18,... | collective-permute-start | bytes 417800 | tf_op jit(solution)/shard_map/ppermute | solution.py:435
  87.2 4.1 %near_attention.2.early_ref = bf16[128,1280]{1,0:T(8,128)(2,1)} custom-call(s32[1]{0:T(128)} %bitcast.2.z_ref, f32[256,64]{1,0:T(8,128)} %get-tuple-element.30.cos_ref, f32[256,64]{1,0:T(8,128)} %get-tuple-element.29.sin_ref, f32[128,64]{1,0:T(8,128)} %get-tuple-element.32.pcos_ref, f32[128,64]{1,0:T(8,128)} %get-tuple-element.31.psin_ref, ...), custom_call_target="tpu_custom_call" | custom-call | flops 1073741824 | bytes 2097152 | tf_op jit(solution)/shard_map/near_attention/pallas_call | solution.py:331
  91.2 0.0 copy-start.2
  91.2 0.0 collective-permute-done.1.refs_0_
  91.3 4.2 %near_attention.3.late_ref = bf16[128,1280]{1,0:T(8,128)(2,1)} custom-call(s32[1]{0:T(128)} %bitcast.2.z_ref, f32[256,64]{1,0:T(8,128)} %get-tuple-element.30.cos_ref, f32[256,64]{1,0:T(8,128)} %get-tuple-element.29.sin_ref, f32[128,64]{1,0:T(8,128)} %get-tuple-element.32.pcos_ref, f32[128,64]{1,0:T(8,128)} %get-tuple-element.31.psin_ref, ...), custom_call_target="tpu_custom_call" | custom-call | flops 1073741824 | bytes 2097152 | tf_op jit(solution)/shard_map/near_attention/pallas_call | solution.py:331
  95.5 0.0 collective-permute-done.10.one_ref
  95.5 0.0 collective-permute-done.11.two_ref
  95.5 0.0 collective-permute-done.12.three_ref
  95.5 0.0 all-to-all-done.1.far_ref
  95.5 0.0 copy-done.2
  95.5 0.0 copy-start.3
  95.5 1.0 copy-done.3
  96.5 1.8 %merge_groups.1.in_ref = bf16[256,1024]{1,0:T(8,128)(2,1)S(1)} custom-call(s32[1]{0:T(128)} %bitcast.1.x_ref, bf16[128,1280]{1,0:T(8,128)(2,1)S(1)} %copy-done.2, bf16[128,1280]{1,0:T(8,128)(2,1)S(1)} %copy-done.3, bf16[16,144,128]{2,1,0:T(8,128)(2,1)S(1)} %all-to-all-done.1.far_ref, bf16[2,272,128]{2,1,0:T(8,128)(2,1)S(1)} %get-tuple-element.25.own_ref, ...), custom_call_target="tpu_custom_call" | custom-call | flops 16777216 | bytes 2097152 | tf_op jit(solution)/shard_map/merge_groups/pallas_call | solution.py:385
  98.3 10.5 %collective-permute-start.13 = (bf16[256,1024]{1,0:T(8,128)(2,1)S(1)}, bf16[256,1024]{1,0:T(8,128)(2,1)S(1)}, u32[]{:S(2)}, u32[]{:S(2)}) collective-permute-start(bf16[256,1024]{1,0:T(8,128)(2,1)S(1)} %merge_groups.1.in_ref), channel_id=1, source_target_pairs={{0,1},{1,0},{2,3},{3,2},{4,5},{5,4},{6,7},{7,6},{8,9},{9,8},{10,11... | collective-permute-start | bytes 1572872 | tf_op jit(solution)/shard_map/ppermute | solution.py:466
  108.8 2.2 %copy-done = bf16[2048,1024]{1,0:T(8,128)(2,1)S(1)} copy-done((bf16[2048,1024]{1,0:T(8,128)(2,1)S(1)}, bf16[2048,1024]{1,0:T(8,128)(2,1)}, u32[]{:S(2)}) %copy-start) | copy-done | bytes 4194328
  111.0 0.7 project.2.refs_0_
  111.7 0.0 collective-permute-done.13.in_ref
  111.7 1.5 %copy-done.1 = bf16[2048,1024]{1,0:T(8,128)(2,1)S(1)} copy-done((bf16[2048,1024]{1,0:T(8,128)(2,1)S(1)}, bf16[2048,1024]{1,0:T(8,128)(2,1)}, u32[]{:S(2)}) %copy-start.1) | copy-done | bytes 4194328
  113.2 1.5 %project.3 = bf16[256,1024]{1,0:T(8,128)(2,1)} custom-call(s32[1]{0:T(128)S(6)} %sub.13.core_ref, bf16[256,1024]{1,0:T(8,128)(2,1)S(1)} %collective-permute-done.13.in_ref, bf16[2048,1024]{1,0:T(8,128)(2,1)S(1)} %copy-done.1, f32[256,1024]{1,0:T(8,128)S(1)} %project.2.refs_0_), custom_call_target="tpu_custom_call" | custom-call | flops 536870912 | bytes 4194304 | tf_op jit(solution)/shard_map/project/pallas_call | solution.py:409
  (7 shorter events, 0.1 us)
Async XLA Ops:
  5.8 30.9 %all-to-all-start = ((bf16[16,3,128,128]{3,2,1,0:T(8,128)(2,1)}), bf16[16,3,128,128]{3,2,1,0:T(8,128)(2,1)S(1)}, u32[]{:S(2)}, u32[]{:S(2)}) async-start(bf16[16,3,128,128]{3,2,1,0:T(8,128)(2,1)} %plane_pieces.1), calls=%async_computation | async-start | bytes 3145728 | tf_op jit(solution)/shard_map/all_to_all | solution.py:447
  14.5 30.3 %copy-start.7 = (bf16[1,128,1024]{2,1,0:T(8,128)(2,1)}, bf16[1,128,1024]{2,1,0:T(8,128)(2,1)S(1)}, u32[]{:S(2)}) copy-start(bf16[1,128,1024]{2,1,0:T(8,128)(2,1)S(1)} %slice.9) | copy-start | bytes 786436
  15.4 43.2 %collective-permute-start = (bf16[2,128,1024]{2,1,0:T(8,128)(2,1)}, bf16[2,128,1024]{2,1,0:T(8,128)(2,1)}, u32[]{:S(2)}, u32[]{:S(2)}) collective-permute-start(bf16[2,128,1024]{2,1,0:T(8,128)(2,1)} %pad_maximum_fusion), channel_id=1, source_target_pairs={{6,14},{14,22},{22,30},{30,38},{38,46},{46,54},{54,62},{62,70},{70... | collective-permute-start | bytes 1572872 | tf_op jit(solution)/shard_map/ppermute | solution.py:452
  37.5 27.0 %collective-permute-start.2 = (bf16[8,2,128,128]{3,2,1,0:T(8,128)(2,1)}, bf16[8,2,128,128]{3,2,1,0:T(8,128)(2,1)}, u32[]{:S(2)}, u32[]{:S(2)}) collective-permute-start(bf16[8,2,128,128]{3,2,1,0:T(8,128)(2,1)} %slice.12), channel_id=1, source_target_pairs={{0,32},{2,34},{4,36},{6,38},{8,40},{10,42},{12,44},{14,46},{16,48}... | collective-permute-start | bytes 1572872 | tf_op jit(solution)/shard_map/ppermute | solution.py:438
  44.8 6.7 %collective-permute-start.3 = (bf16[2,2,256,128]{3,2,1,0:T(8,128)(2,1)}, bf16[2,2,256,128]{3,2,1,0:T(8,128)(2,1)S(1)}, u32[]{:S(2)}, u32[]{:S(2)}) collective-permute-start(bf16[2,2,256,128]{3,2,1,0:T(8,128)(2,1)} %get-tuple-element.18), channel_id=1, source_target_pairs={{0,2},{2,4},{4,6},{6,0},{8,10},{10,12},{12,14},{14,8},{16,18},{18,... | collective-permute-start | bytes 786440 | tf_op jit(solution)/shard_map/ppermute | solution.py:435
  44.9 10.1 %collective-permute-start.4 = (bf16[2,2,256,128]{3,2,1,0:T(8,128)(2,1)}, bf16[2,2,256,128]{3,2,1,0:T(8,128)(2,1)S(1)}, u32[]{:S(2)}, u32[]{:S(2)}) collective-permute-start(bf16[2,2,256,128]{3,2,1,0:T(8,128)(2,1)} %get-tuple-element.19), channel_id=1, source_target_pairs={{0,4},{2,6},{4,0},{6,2},{8,12},{10,14},{12,8},{14,10},{16,20},{18,... | collective-permute-start | bytes 786440 | tf_op jit(solution)/shard_map/ppermute | solution.py:435
  48.1 9.4 %collective-permute-start.5 = (bf16[2,2,256,128]{3,2,1,0:T(8,128)(2,1)}, bf16[2,2,256,128]{3,2,1,0:T(8,128)(2,1)S(1)}, u32[]{:S(2)}, u32[]{:S(2)}) collective-permute-start(bf16[2,2,256,128]{3,2,1,0:T(8,128)(2,1)} %get-tuple-element.20), channel_id=1, source_target_pairs={{0,6},{2,0},{4,2},{6,4},{8,14},{10,8},{12,10},{14,12},{16,22},{18,... | collective-permute-start | bytes 786440 | tf_op jit(solution)/shard_map/ppermute | solution.py:435
  51.5 27.2 %collective-permute-start.6 = (bf16[2,256,128]{2,1,0:T(8,128)(2,1)}, bf16[2,256,128]{2,1,0:T(8,128)(2,1)S(1)}, u32[]{:S(2)}, u32[]{:S(2)}) collective-permute-start(bf16[2,256,128]{2,1,0:T(8,128)(2,1)} %get-tuple-element.22), channel_id=1, source_target_pairs={{0,2},{2,4},{4,6},{6,0},{8,10},{10,12},{12,14},{14,8},{16,18},{18,... | collective-permute-start | bytes 393224 | tf_op jit(solution)/shard_map/ppermute | solution.py:435
  54.9 23.8 %collective-permute-start.7 = (bf16[2,256,128]{2,1,0:T(8,128)(2,1)}, bf16[2,256,128]{2,1,0:T(8,128)(2,1)S(1)}, u32[]{:S(2)}, u32[]{:S(2)}) collective-permute-start(bf16[2,256,128]{2,1,0:T(8,128)(2,1)} %get-tuple-element.23), channel_id=1, source_target_pairs={{0,4},{2,6},{4,0},{6,2},{8,12},{10,14},{12,8},{14,10},{16,20},{18,... | collective-permute-start | bytes 393224 | tf_op jit(solution)/shard_map/ppermute | solution.py:435
  57.5 21.2 %collective-permute-start.8 = (bf16[2,256,128]{2,1,0:T(8,128)(2,1)}, bf16[2,256,128]{2,1,0:T(8,128)(2,1)}, u32[]{:S(2)}, u32[]{:S(2)}) collective-permute-start(bf16[2,256,128]{2,1,0:T(8,128)(2,1)} %get-tuple-element.24), channel_id=1, source_target_pairs={{0,6},{2,0},{4,2},{6,4},{8,14},{10,8},{12,10},{14,12},{16,22},{18,... | collective-permute-start | bytes 393224 | tf_op jit(solution)/shard_map/ppermute | solution.py:435
  57.5 1.0 copy-start.4
  58.5 5.0 %copy-start.8 = (bf16[1,128,1024]{2,1,0:T(8,128)(2,1)S(1)}, bf16[1,128,1024]{2,1,0:T(8,128)(2,1)}, u32[]{:S(2)}) copy-start(bf16[1,128,1024]{2,1,0:T(8,128)(2,1)} %copy-done.7) | copy-start | bytes 786436
  58.5 20.2 %collective-permute-start.9 = (bf16[2,2,2,256,128]{4,3,2,1,0:T(8,128)(2,1)S(1)}, bf16[2,2,2,256,128]{4,3,2,1,0:T(8,128)(2,1)}, u32[]{:S(2)}, u32[]{:S(2)}) collective-permute-start(bf16[2,2,2,256,128]{4,3,2,1,0:T(8,128)(2,1)S(1)} %pick_last.1), channel_id=1, source_target_pairs={{0,8},{2,10},{4,12},{6,14},{8,16},{10,18},{12,20},{14,22},{16,24},... | collective-permute-start | bytes 1572872 | tf_op jit(solution)/shard_map/ppermute | solution.py:438
  64.4 26.8 %collective-permute-start.1 = (bf16[2,128,1024]{2,1,0:T(8,128)(2,1)}, bf16[2,128,1024]{2,1,0:T(8,128)(2,1)}, u32[]{:S(2)}, u32[]{:S(2)}) collective-permute-start(bf16[2,128,1024]{2,1,0:T(8,128)(2,1)} %broadcast_select_fusion), channel_id=1, source_target_pairs={{0,2},{2,4},{4,6},{6,0},{8,10},{10,12},{12,14},{14,8},{16,18},{18,... | collective-permute-start | bytes 1572872 | tf_op jit(solution)/shard_map/ppermute | solution.py:435
  64.4 14.3 %copy-start.5 = (bf16[2,2,256,128]{3,2,1,0:T(8,128)(2,1)S(1)}, bf16[2,2,256,128]{3,2,1,0:T(8,128)(2,1)}, u32[]{:S(2)}) copy-start(bf16[2,2,256,128]{3,2,1,0:T(8,128)(2,1)} %get-tuple-element.17.own_ref.refs_0_) | copy-start | bytes 786436
  64.4 14.3 %copy-start.6 = (bf16[2,256,128]{2,1,0:T(8,128)(2,1)S(1)}, bf16[2,256,128]{2,1,0:T(8,128)(2,1)}, u32[]{:S(2)}) copy-start(bf16[2,256,128]{2,1,0:T(8,128)(2,1)} %get-tuple-element.21.refs_4_) | copy-start | bytes 393220
  68.0 27.5 %all-to-all-start.1 = ((bf16[16,144,128]{2,1,0:T(8,128)(2,1)}), bf16[16,144,128]{2,1,0:T(8,128)(2,1)S(1)}, u32[]{:S(2)}, u32[]{:S(2)}) async-start(bf16[16,144,128]{2,1,0:T(8,128)(2,1)} %plane_attention.1), calls=%async_computation.1 | async-start | bytes 1179648 | tf_op jit(solution)/shard_map/all_to_all | solution.py:462
  82.1 13.3 %collective-permute-start.10 = (bf16[2,272,128]{2,1,0:T(8,128)(2,1)S(1)}, bf16[2,272,128]{2,1,0:T(8,128)(2,1)S(1)}, u32[]{:S(2)}, u32[]{:S(2)}) collective-permute-start(bf16[2,272,128]{2,1,0:T(8,128)(2,1)S(1)} %get-tuple-element.26), channel_id=1, source_target_pairs={{0,2},{2,4},{4,6},{6,0},{8,10},{10,12},{12,14},{14,8},{16,18},{18,... | collective-permute-start | bytes 417800 | tf_op jit(solution)/shard_map/ppermute | solution.py:435
  83.6 11.9 %collective-permute-start.11 = (bf16[2,272,128]{2,1,0:T(8,128)(2,1)S(1)}, bf16[2,272,128]{2,1,0:T(8,128)(2,1)S(1)}, u32[]{:S(2)}, u32[]{:S(2)}) collective-permute-start(bf16[2,272,128]{2,1,0:T(8,128)(2,1)S(1)} %get-tuple-element.27), channel_id=1, source_target_pairs={{0,4},{2,6},{4,0},{6,2},{8,12},{10,14},{12,8},{14,10},{16,20},{18,... | collective-permute-start | bytes 417800 | tf_op jit(solution)/shard_map/ppermute | solution.py:435
  86.0 9.5 %collective-permute-start.12 = (bf16[2,272,128]{2,1,0:T(8,128)(2,1)S(1)}, bf16[2,272,128]{2,1,0:T(8,128)(2,1)S(1)}, u32[]{:S(2)}, u32[]{:S(2)}) collective-permute-start(bf16[2,272,128]{2,1,0:T(8,128)(2,1)S(1)} %get-tuple-element.28), channel_id=1, source_target_pairs={{0,6},{2,0},{4,2},{6,4},{8,14},{10,8},{12,10},{14,12},{16,22},{18,... | collective-permute-start | bytes 417800 | tf_op jit(solution)/shard_map/ppermute | solution.py:435
  91.2 4.3 %copy-start.2 = (bf16[128,1280]{1,0:T(8,128)(2,1)S(1)}, bf16[128,1280]{1,0:T(8,128)(2,1)}, u32[]{:S(2)}) copy-start(bf16[128,1280]{1,0:T(8,128)(2,1)} %near_attention.2.early_ref) | copy-start | bytes 983044
  95.5 1.0 copy-start.3
  98.3 13.4 %collective-permute-start.13 = (bf16[256,1024]{1,0:T(8,128)(2,1)S(1)}, bf16[256,1024]{1,0:T(8,128)(2,1)S(1)}, u32[]{:S(2)}, u32[]{:S(2)}) collective-permute-start(bf16[256,1024]{1,0:T(8,128)(2,1)S(1)} %merge_groups.1.in_ref), channel_id=1, source_target_pairs={{0,1},{1,0},{2,3},{3,2},{4,5},{5,4},{6,7},{7,6},{8,9},{9,8},{10,11... | collective-permute-start | bytes 1572872 | tf_op jit(solution)/shard_map/ppermute | solution.py:466
  108.8 2.2 %copy-start = (bf16[2048,1024]{1,0:T(8,128)(2,1)S(1)}, bf16[2048,1024]{1,0:T(8,128)(2,1)}, u32[]{:S(2)}) copy-start(bf16[2048,1024]{1,0:T(8,128)(2,1)} %w_ref.3) | copy-start | bytes 12582916
  111.0 2.2 %copy-start.1 = (bf16[2048,1024]{1,0:T(8,128)(2,1)S(1)}, bf16[2048,1024]{1,0:T(8,128)(2,1)}, u32[]{:S(2)}) copy-start(bf16[2048,1024]{1,0:T(8,128)(2,1)} %w_ref.3) | copy-start | bytes 12582916

commit v3 on v2

--- a/solution.py
+++ b/solution.py
@@ -394,27 +394,25 @@
     )(x, early, late, far, own, *others)
 
 
-def project_kernel(core_ref, in_ref, w_ref, *refs):
+def project_kernel(in_ref, w_ref, *refs):
     *partial, out_ref = refs
-    half = LOCAL * HEAD
-    rows = pl.ds(pl.multiple_of(core_ref[0] * half, half), half)
-    total = jnp.dot(in_ref[...], w_ref[rows, :], preferred_element_type=f32)
+    total = jnp.dot(in_ref[...], w_ref[...], preferred_element_type=f32)
     if partial:
         total += partial[0][...]
     out_ref[...] = total.astype(out_ref.dtype)
 
 
-def project(core, block, w_out, partial, dtype):
+def project(block, w_out, partial, dtype):
     vmem = pl.BlockSpec(memory_space=pltpu.VMEM)
     return pl.pallas_call(
         project_kernel,
-        in_specs=[pl.BlockSpec(memory_space=pltpu.SMEM)] + [vmem] * (2 + len(partial)),
+        in_specs=[vmem] * (2 + len(partial)),
         out_specs=vmem,
         out_shape=jax.ShapeDtypeStruct((TOKENS, w_out.shape[1]), dtype),
         compiler_params=pltpu.CompilerParams(vmem_limit_bytes=8 * 2**20),
         cost_estimate=pl.CostEstimate(flops=2**29, bytes_accessed=2**22, transcendentals=0),
         name="project",
-    )(core, block, w_out, *partial)
+    )(block, w_out, *partial)
 
 
 def tables(count, start):
@@ -438,7 +436,8 @@
         return lax.ppermute(block, "sp", [(i, i + distance) for i in range(devices - distance)])
 
     device = lax.axis_index("sp")
-    core = lax.axis_index("tp").reshape(1)
+    core = lax.axis_index("tp")
+    width = LOCAL * HEAD
     x = lax.rem(device, ROW).reshape(1)
     start = device * TOKENS
     cosine, sine = tables(TOKENS, start)
@@ -454,6 +453,8 @@
     edge = along_row(jnp.where(x[0] == ROW - 1, up, edge), 1)
     last = pick_last(x, pieces)
     halo1 = onward(last, ROW)
+    w_mine = lax.dynamic_slice_in_dim(w_out, core * width, width)
+    w_other = lax.dynamic_slice_in_dim(w_out, (1 - core) * width, width)
     pcos, psin = tables(HALF, start - HALF)
     near_args = (device.reshape(1), cosine, sine, pcos, psin, queries, keys, values, edge)
     early = near_attention(1, *near_args)
@@ -464,8 +465,8 @@
     back = [along_row(block, steps) for steps, block in enumerate(sent, 1)]
     attended = merge_groups(x, early, late, far, mine, back)
     other = lax.ppermute(attended, "tp", [(0, 1), (1, 0)])
-    partial = project(core, attended, w_out, (), f32)
-    return project(1 - core, other, w_out, (partial,), bf16)
+    partial = project(attended, w_mine, (), f32)
+    return project(other, w_other, (partial,), bf16)
 
 
 def solution(mesh):

time: 115 us -> 115 us (level)
    unnamed x18 -> x12, local copies, waits for them, and re-layouts: 5.59 us -> 1.93 us
    dynamic_slice x0 -> x1, local copies, waits for them, and re-layouts: none -> 2.66 us  [shards(): w_mine = lax.dynamic_slice_in_dim(w_out, core * width, width)]
  transfers between devices with their start and end apart: 16 -> 16, of which waited for: 3 -> 3; matrix products, arithmetic and copies ran while one was open for 5% -> 8% of each run, Pallas kernels for 17% -> 17%
where the time goes in v3:
time: 115 us; the launch traced here: 114 us
  starting transfers between devices  47.6 us (41%)
  Pallas kernels  27.5 us (24%)
  waiting for transfers between devices  26.6 us (23%)
  local copies, waits for them, and re-layouts  7.37 us (6%)
  other arithmetic  4.98 us (4%)
    all_to_all x1, waiting for transfers between devices, shards(): held = exchange(held)  19.8 us
    ppermute x10, starting transfers between devices, along_row(): lax.ppermute(block, 'sp', [(i, i // ROW * ROW + (i + steps) % ROW) for i...  11 us
    ppermute x1, starting transfers between devices, shards(): other = lax.ppermute(attended, 'tp', [(0, 1), (1, 0)])  10.2 us
    all_to_all x1, starting transfers between devices, shards(): far = exchange(far)  9.61 us
    ppermute x2, starting transfers between devices, onward(): lax.ppermute(block, 'sp', [(i, i + distance) for i in range(devices - dis...  8.51 us
    pallas_call x2, Pallas kernels, near_attention(): pl.pallas_call(functools.partial(near_kernel, half), in_specs=[pl.BlockSp...  8.27 us
    ppermute x10, waiting for transfers between devices, along_row(): lax.ppermute(block, 'sp', [(i, i // ROW * ROW + (i + steps) % ROW) for i...  6.78 us
    all_to_all x1, starting transfers between devices, shards(): held = exchange(held)  6.77 us
  transfers between devices with their start and end apart: 16, of which 3 were waited for; matrix products, arithmetic and copies ran while one was open for 8% of the time, Pallas kernels for 17%

profile of v3, /device:TPU:65, one launch (start us, length us, event | category | flops | bytes accessed | tf_op | source)
XLA Modules:
  0.0 114.3 jit_solution(14305590513389653575)
XLA Ops:
  0.0 1.2 %multiply_sine_fusion = (f32[256,64]{1,0:T(8,128)}, f32[256,64]{1,0:T(8,128)}) fusion(f32[64]{0:T(128)S(1)} %multiply_power_fusion, f32[256]{0:T(256)S(1)} %add_convert_fusion), kind=kLoop, calls=%fused_computation.2 | loop fusion | flops 16384 | bytes 132352 | tf_op jit(solution)/shard_map/sin | solution.py:421
  1.3 4.5 %plane_pieces.1 = bf16[16,3,128,128]{3,2,1,0:T(8,128)(2,1)} custom-call(f32[256,64]{1,0:T(8,128)} %get-tuple-element.32.cos_ref, f32[256,64]{1,0:T(8,128)} %get-tuple-element.31.sin_ref, bf16[3,256,1024]{2,1,0:T(8,128)(2,1)} %k_ref.3, bf16[3,256,1024]{2,1,0:T(8,128)(2,1)} %v_ref.3, bf16[3,256,1024]{2,1,0:T(8,128)(2,1)} %q_ref.3), custom_call_target="tpu_custom_call" | custom-call | flops 1073741824 | bytes 3145728 | tf_op jit(solution)/shard_map/plane_pieces/pallas_call | solution.py:78
  5.7 6.8 %all-to-all-start = ((bf16[16,3,128,128]{3,2,1,0:T(8,128)(2,1)}), bf16[16,3,128,128]{3,2,1,0:T(8,128)(2,1)S(1)}, u32[]{:S(2)}, u32[]{:S(2)}) async-start(bf16[16,3,128,128]{3,2,1,0:T(8,128)(2,1)} %plane_pieces.1), calls=%async_computation | async-start | bytes 3145728 | tf_op jit(solution)/shard_map/all_to_all | solution.py:446
  12.5 1.0 slice.10
  13.5 1.0 slice.9
  14.5 0.0 copy-start.5
  14.5 0.9 pad_maximum_fusion
  15.3 1.5 %collective-permute-start = (bf16[2,128,1024]{2,1,0:T(8,128)(2,1)}, bf16[2,128,1024]{2,1,0:T(8,128)(2,1)}, u32[]{:S(2)}, u32[]{:S(2)}) collective-permute-start(bf16[2,128,1024]{2,1,0:T(8,128)(2,1)} %pad_maximum_fusion), channel_id=1, source_target_pairs={{6,14},{14,22},{22,30},{30,38},{38,46},{46,54},{54,62},{62,70},{70... | collective-permute-start | bytes 1572872 | tf_op jit(solution)/shard_map/ppermute | solution.py:451
  16.8 19.8 %all-to-all-done.in_ref = bf16[16,3,128,128]{3,2,1,0:T(8,128)(2,1)S(1)} async-done(((bf16[16,3,128,128]{3,2,1,0:T(8,128)(2,1)}), bf16[16,3,128,128]{3,2,1,0:T(8,128)(2,1)S(1)}, u32[]{:S(2)}, u32[]{:S(2)}) %all-to-all-start) | async-done | bytes 1572896 | tf_op jit(solution)/shard_map/all_to_all | solution.py:446
  36.6 0.8 slice.12
  37.4 3.5 %collective-permute-start.2 = (bf16[8,2,128,128]{3,2,1,0:T(8,128)(2,1)}, bf16[8,2,128,128]{3,2,1,0:T(8,128)(2,1)}, u32[]{:S(2)}, u32[]{:S(2)}) collective-permute-start(bf16[8,2,128,128]{3,2,1,0:T(8,128)(2,1)} %slice.12), channel_id=1, source_target_pairs={{0,32},{2,34},{4,36},{6,38},{8,40},{10,42},{12,44},{14,46},{16,48}... | collective-permute-start | bytes 1572872 | tf_op jit(solution)/shard_map/ppermute | solution.py:436
  41.0 3.8 %row_pieces.1 = (bf16[2,2,256,128]{3,2,1,0:T(8,128)(2,1)}, bf16[2,2,256,128]{3,2,1,0:T(8,128)(2,1)}, bf16[2,2,256,128]{3,2,1,0:T(8,128)(2,1)}, bf16[2,2,256,128]...) custom-call(s32[1]{0:T(128)} %bitcast.x_ref, ...), custom_call_target="tpu_custom_call" | custom-call | flops 1073741824 | bytes 3145728 | tf_op jit(solution)/shard_map/row_pieces/pallas_call | solution.py:124
  44.7 0.0 copy-done.5
  44.8 0.1 collective-permute-start.3
  44.8 3.3 %collective-permute-start.4 = (bf16[2,2,256,128]{3,2,1,0:T(8,128)(2,1)}, bf16[2,2,256,128]{3,2,1,0:T(8,128)(2,1)S(1)}, u32[]{:S(2)}, u32[]{:S(2)}) collective-permute-start(bf16[2,2,256,128]{3,2,1,0:T(8,128)(2,1)} %get-tuple-element.19), channel_id=1, source_target_pairs={{0,4},{2,6},{4,0},{6,2},{8,12},{10,14},{12,8},{14,10},{16,20},{18,... | collective-permute-start | bytes 786440 | tf_op jit(solution)/shard_map/ppermute | solution.py:433
  48.1 0.0 collective-permute-start.5
  48.1 3.3 %collective-permute-done.3.one_ref.refs_1_ = bf16[2,2,256,128]{3,2,1,0:T(8,128)(2,1)S(1)} collective-permute-done((bf16[2,2,256,128]{3,2,1,0:T(8,128)(2,1)}, bf16[2,2,256,128]{3,2,1,0:T(8,128)(2,1)S(1)}, u32[]{:S(2)}, u32[]{:S(2)}) %collective-permute-start.3) | collective-permute-done | bytes 262176 | tf_op jit(solution)/shard_map/ppermute | solution.py:433
  51.5 0.0 collective-permute-start.6
  51.5 3.4 %collective-permute-done.4.two_ref.refs_2_ = bf16[2,2,256,128]{3,2,1,0:T(8,128)(2,1)S(1)} collective-permute-done((bf16[2,2,256,128]{3,2,1,0:T(8,128)(2,1)}, bf16[2,2,256,128]{3,2,1,0:T(8,128)(2,1)S(1)}, u32[]{:S(2)}, u32[]{:S(2)}) %collective-permute-start.4) | collective-permute-done | bytes 262176 | tf_op jit(solution)/shard_map/ppermute | solution.py:433
  54.9 2.6 %collective-permute-start.7 = (bf16[2,256,128]{2,1,0:T(8,128)(2,1)}, bf16[2,256,128]{2,1,0:T(8,128)(2,1)S(1)}, u32[]{:S(2)}, u32[]{:S(2)}) collective-permute-start(bf16[2,256,128]{2,1,0:T(8,128)(2,1)} %get-tuple-element.23), channel_id=1, source_target_pairs={{0,4},{2,6},{4,0},{6,2},{8,12},{10,14},{12,8},{14,10},{16,20},{18,... | collective-permute-start | bytes 393224 | tf_op jit(solution)/shard_map/ppermute | solution.py:433
  57.5 0.0 collective-permute-done.5.three_ref.refs_3_
  57.5 0.0 collective-permute-start.8
  57.5 0.0 copy-start.2
  57.5 0.9 copy-done.2
  58.5 0.0 collective-permute-done
  58.5 5.0 %collective-permute-start.9 = (bf16[2,2,2,256,128]{4,3,2,1,0:T(8,128)(2,1)S(1)}, bf16[2,2,2,256,128]{4,3,2,1,0:T(8,128)(2,1)}, u32[]{:S(2)}, u32[]{:S(2)}) collective-permute-start(bf16[2,2,2,256,128]{4,3,2,1,0:T(8,128)(2,1)S(1)} %pick_last.1), channel_id=1, source_target_pairs={{0,8},{2,10},{4,12},{6,14},{8,16},{10,18},{12,20},{14,22},{16,24},... | collective-permute-start | bytes 1572872 | tf_op jit(solution)/shard_map/ppermute | solution.py:436
  63.5 1.8 %broadcast_select_fusion = bf16[2,128,1024]{2,1,0:T(8,128)(2,1)} fusion(bf16[2,128,1024]{2,1,0:T(8,128)(2,1)} %collective-permute-done, pred[]{:T(512)S(6)} %eq.3, bf16[1,128,1024]{2,1,0:T(8,128)(2,1)S(1)} %slice.10, bf16[1,128,1024]{2,1,0:T(8,128)(2,1)} %copy-done.5), kind=kLoop, calls=%fused_computation.1 | loop fusion | flops 524288 | bytes 1572865 | tf_op jit(solution)/shard_map/jit(_where)/select_n | solution.py:453
  65.3 0.0 collective-permute-done.2.halo_ref
  65.3 0.0 collective-permute-start.1
  65.3 0.0 copy-start.3
  65.3 0.0 copy-start.4
  65.3 3.6 %plane_attention.1 = bf16[16,144,128]{2,1,0:T(8,128)(2,1)} custom-call(s32[1]{0:T(128)} %bitcast.2.z_ref, bf16[16,3,128,128]{3,2,1,0:T(8,128)(2,1)S(1)} %all-to-all-done.in_ref, bf16[8,2,128,128]{3,2,1,0:T(8,128)(2,1)} %collective-permute-done.2.halo_ref), custom_call_target="tpu_custom_call" | custom-call | flops 2147483648 | bytes 3145728 | tf_op jit(solution)/shard_map/plane_attention/pallas_call | solution.py:207
  68.9 9.6 %all-to-all-start.1 = ((bf16[16,144,128]{2,1,0:T(8,128)(2,1)}), bf16[16,144,128]{2,1,0:T(8,128)(2,1)S(1)}, u32[]{:S(2)}, u32[]{:S(2)}) async-start(bf16[16,144,128]{2,1,0:T(8,128)(2,1)} %plane_attention.1), calls=%async_computation.1 | async-start | bytes 1179648 | tf_op jit(solution)/shard_map/all_to_all | solution.py:463
  78.6 1.0 multiply_sine_fusion.1
  79.5 0.1 pad_add_fusion.x_ref
  79.6 0.0 collective-permute-done.6.refs_5_
  79.6 0.0 collective-permute-done.7.refs_6_
  79.6 0.0 collective-permute-done.8.refs_7_
  79.6 0.0 collective-permute-done.9.refs_8_
  79.6 0.0 copy-done.3
  79.6 0.0 copy-done.4
  79.6 3.3 %row_attention.1 = (bf16[2,272,128]{2,1,0:T(8,128)(2,1)S(1)}, bf16[2,272,128]{2,1,0:T(8,128)(2,1)S(1)}, bf16[2,272,128]{2,1,0:T(8,128)(2,1)S(1)}, bf16[2,272,128]{2,1,0:T(8,128)(2,1)S(1)}) custom-call(s32[2]{0:T(128)S(1)} %pad_add_fusion.x_ref, bf16[2,2,256,128]{3,2,1,0:T(8,128)(2,1)S(1)} %copy-done.3, ...), custom_call_target="tpu_custom_call" | custom-call | flops 2147483648 | bytes 3145728 | tf_op jit(solution)/shard_map/row_attention/pallas_call | solution.py:277
  83.0 1.4 %collective-permute-start.10 = (bf16[2,272,128]{2,1,0:T(8,128)(2,1)S(1)}, bf16[2,272,128]{2,1,0:T(8,128)(2,1)S(1)}, u32[]{:S(2)}, u32[]{:S(2)}) collective-permute-start(bf16[2,272,128]{2,1,0:T(8,128)(2,1)S(1)} %get-tuple-element.26), channel_id=1, source_target_pairs={{0,2},{2,4},{4,6},{6,0},{8,10},{10,12},{12,14},{14,8},{16,18},{18,... | collective-permute-start | bytes 417800 | tf_op jit(solution)/shard_map/ppermute | solution.py:433
  84.4 2.4 %collective-permute-start.11 = (bf16[2,272,128]{2,1,0:T(8,128)(2,1)S(1)}, bf16[2,272,128]{2,1,0:T(8,128)(2,1)S(1)}, u32[]{:S(2)}, u32[]{:S(2)}) collective-permute-start(bf16[2,272,128]{2,1,0:T(8,128)(2,1)S(1)} %get-tuple-element.27), channel_id=1, source_target_pairs={{0,4},{2,6},{4,0},{6,2},{8,12},{10,14},{12,8},{14,10},{16,20},{18,... | collective-permute-start | bytes 417800 | tf_op jit(solution)/shard_map/ppermute | solution.py:433
  86.9 1.2 %collective-permute-start.12 = (bf16[2,272,128]{2,1,0:T(8,128)(2,1)S(1)}, bf16[2,272,128]{2,1,0:T(8,128)(2,1)S(1)}, u32[]{:S(2)}, u32[]{:S(2)}) collective-permute-start(bf16[2,272,128]{2,1,0:T(8,128)(2,1)S(1)} %get-tuple-element.28), channel_id=1, source_target_pairs={{0,6},{2,0},{4,2},{6,4},{8,14},{10,8},{12,10},{14,12},{16,22},{18,... | collective-permute-start | bytes 417800 | tf_op jit(solution)/shard_map/ppermute | solution.py:433
  88.0 4.1 %near_attention.2.early_ref = bf16[128,1280]{1,0:T(8,128)(2,1)} custom-call(s32[1]{0:T(128)} %bitcast.1.z_ref, f32[256,64]{1,0:T(8,128)} %get-tuple-element.32.cos_ref, f32[256,64]{1,0:T(8,128)} %get-tuple-element.31.sin_ref, f32[128,64]{1,0:T(8,128)} %get-tuple-element.34.pcos_ref, f32[128,64]{1,0:T(8,128)} %get-tuple-element.33.psin_ref, ...), custom_call_target="tpu_custom_call" | custom-call | flops 1073741824 | bytes 2097152 | tf_op jit(solution)/shard_map/near_attention/pallas_call | solution.py:331
  92.1 0.0 copy-start
  92.1 0.0 collective-permute-done.1.refs_0_
  92.1 4.2 %near_attention.3.late_ref = bf16[128,1280]{1,0:T(8,128)(2,1)} custom-call(s32[1]{0:T(128)} %bitcast.1.z_ref, f32[256,64]{1,0:T(8,128)} %get-tuple-element.32.cos_ref, f32[256,64]{1,0:T(8,128)} %get-tuple-element.31.sin_ref, f32[128,64]{1,0:T(8,128)} %get-tuple-element.34.pcos_ref, f32[128,64]{1,0:T(8,128)} %get-tuple-element.33.psin_ref, ...), custom_call_target="tpu_custom_call" | custom-call | flops 1073741824 | bytes 2097152 | tf_op jit(solution)/shard_map/near_attention/pallas_call | solution.py:331
  96.3 0.0 collective-permute-done.10.one_ref
  96.3 0.0 collective-permute-done.11.two_ref
  96.4 0.0 collective-permute-done.12.three_ref
  96.4 0.0 all-to-all-done.1.far_ref
  96.4 0.0 copy-done
  96.4 0.0 copy-start.1
  96.4 1.0 copy-done.1
  97.4 1.8 %merge_groups.1.in_ref = bf16[256,1024]{1,0:T(8,128)(2,1)S(1)} custom-call(s32[1]{0:T(128)} %bitcast.x_ref, bf16[128,1280]{1,0:T(8,128)(2,1)S(1)} %copy-done, bf16[128,1280]{1,0:T(8,128)(2,1)S(1)} %copy-done.1, bf16[16,144,128]{2,1,0:T(8,128)(2,1)S(1)} %all-to-all-done.1.far_ref, bf16[2,272,128]{2,1,0:T(8,128)(2,1)S(1)} %get-tuple-element.25.own_ref, ...), custom_call_target="tpu_custom_call" | custom-call | flops 16777216 | bytes 2097152 | tf_op jit(solution)/shard_map/merge_groups/pallas_call | solution.py:385
  99.2 10.2 %collective-permute-start.13 = (bf16[256,1024]{1,0:T(8,128)(2,1)S(1)}, bf16[256,1024]{1,0:T(8,128)(2,1)S(1)}, u32[]{:S(2)}, u32[]{:S(2)}) collective-permute-start(bf16[256,1024]{1,0:T(8,128)(2,1)S(1)} %merge_groups.1.in_ref), channel_id=1, source_target_pairs={{0,1},{1,0},{2,3},{3,2},{4,5},{5,4},{6,7},{7,6},{8,9},{9,8},{10,11... | collective-permute-start | bytes 1572872 | tf_op jit(solution)/shard_map/ppermute | solution.py:467
  109.4 2.7 %constant_dynamic-slice_fusion = (bf16[1024,1024]{1,0:T(8,128)(2,1)S(1)}, bf16[1024,1024]{1,0:T(8,128)(2,1)S(1)}) fusion(bf16[2048,1024]{1,0:T(8,128)(2,1)} %param.7, s32[]{:T(128)S(6)} %select_n.27, s32[]{:T(128)S(6)} %select_n.26), kind=kLoop, calls=%fused_computation.10 | loop fusion | bytes 8388616 | tf_op jit(solution)/shard_map/dynamic_slice | solution.py:456
  112.1 0.7 project.2.refs_0_
  112.8 0.0 collective-permute-done.13.in_ref
  112.8 1.5 %project.3 = bf16[256,1024]{1,0:T(8,128)(2,1)} custom-call(bf16[256,1024]{1,0:T(8,128)(2,1)S(1)} %collective-permute-done.13.in_ref, bf16[1024,1024]{1,0:T(8,128)(2,1)S(1)} %get-tuple-element.30.w_ref, f32[256,1024]{1,0:T(8,128)S(1)} %project.2.refs_0_), custom_call_target="tpu_custom_call" | custom-call | flops 536870912 | bytes 4194304 | tf_op jit(solution)/shard_map/project/pallas_call | solution.py:407
  (4 shorter events, 0.1 us)
Async XLA Ops:
  5.7 30.9 %all-to-all-start = ((bf16[16,3,128,128]{3,2,1,0:T(8,128)(2,1)}), bf16[16,3,128,128]{3,2,1,0:T(8,128)(2,1)S(1)}, u32[]{:S(2)}, u32[]{:S(2)}) async-start(bf16[16,3,128,128]{3,2,1,0:T(8,128)(2,1)} %plane_pieces.1), calls=%async_computation | async-start | bytes 3145728 | tf_op jit(solution)/shard_map/all_to_all | solution.py:446
  14.5 30.3 %copy-start.5 = (bf16[1,128,1024]{2,1,0:T(8,128)(2,1)}, bf16[1,128,1024]{2,1,0:T(8,128)(2,1)S(1)}, u32[]{:S(2)}) copy-start(bf16[1,128,1024]{2,1,0:T(8,128)(2,1)S(1)} %slice.9) | copy-start | bytes 786436
  15.3 43.2 %collective-permute-start = (bf16[2,128,1024]{2,1,0:T(8,128)(2,1)}, bf16[2,128,1024]{2,1,0:T(8,128)(2,1)}, u32[]{:S(2)}, u32[]{:S(2)}) collective-permute-start(bf16[2,128,1024]{2,1,0:T(8,128)(2,1)} %pad_maximum_fusion), channel_id=1, source_target_pairs={{6,14},{14,22},{22,30},{30,38},{38,46},{46,54},{54,62},{62,70},{70... | collective-permute-start | bytes 1572872 | tf_op jit(solution)/shard_map/ppermute | solution.py:451
  37.4 27.9 %collective-permute-start.2 = (bf16[8,2,128,128]{3,2,1,0:T(8,128)(2,1)}, bf16[8,2,128,128]{3,2,1,0:T(8,128)(2,1)}, u32[]{:S(2)}, u32[]{:S(2)}) collective-permute-start(bf16[8,2,128,128]{3,2,1,0:T(8,128)(2,1)} %slice.12), channel_id=1, source_target_pairs={{0,32},{2,34},{4,36},{6,38},{8,40},{10,42},{12,44},{14,46},{16,48}... | collective-permute-start | bytes 1572872 | tf_op jit(solution)/shard_map/ppermute | solution.py:436
  44.8 6.7 %collective-permute-start.3 = (bf16[2,2,256,128]{3,2,1,0:T(8,128)(2,1)}, bf16[2,2,256,128]{3,2,1,0:T(8,128)(2,1)S(1)}, u32[]{:S(2)}, u32[]{:S(2)}) collective-permute-start(bf16[2,2,256,128]{3,2,1,0:T(8,128)(2,1)} %get-tuple-element.18), channel_id=1, source_target_pairs={{0,2},{2,4},{4,6},{6,0},{8,10},{10,12},{12,14},{14,8},{16,18},{18,... | collective-permute-start | bytes 786440 | tf_op jit(solution)/shard_map/ppermute | solution.py:433
  44.8 10.1 %collective-permute-start.4 = (bf16[2,2,256,128]{3,2,1,0:T(8,128)(2,1)}, bf16[2,2,256,128]{3,2,1,0:T(8,128)(2,1)S(1)}, u32[]{:S(2)}, u32[]{:S(2)}) collective-permute-start(bf16[2,2,256,128]{3,2,1,0:T(8,128)(2,1)} %get-tuple-element.19), channel_id=1, source_target_pairs={{0,4},{2,6},{4,0},{6,2},{8,12},{10,14},{12,8},{14,10},{16,20},{18,... | collective-permute-start | bytes 786440 | tf_op jit(solution)/shard_map/ppermute | solution.py:433
  48.1 9.4 %collective-permute-start.5 = (bf16[2,2,256,128]{3,2,1,0:T(8,128)(2,1)}, bf16[2,2,256,128]{3,2,1,0:T(8,128)(2,1)S(1)}, u32[]{:S(2)}, u32[]{:S(2)}) collective-permute-start(bf16[2,2,256,128]{3,2,1,0:T(8,128)(2,1)} %get-tuple-element.20), channel_id=1, source_target_pairs={{0,6},{2,0},{4,2},{6,4},{8,14},{10,8},{12,10},{14,12},{16,22},{18,... | collective-permute-start | bytes 786440 | tf_op jit(solution)/shard_map/ppermute | solution.py:433
  51.5 28.1 %collective-permute-start.6 = (bf16[2,256,128]{2,1,0:T(8,128)(2,1)}, bf16[2,256,128]{2,1,0:T(8,128)(2,1)S(1)}, u32[]{:S(2)}, u32[]{:S(2)}) collective-permute-start(bf16[2,256,128]{2,1,0:T(8,128)(2,1)} %get-tuple-element.22), channel_id=1, source_target_pairs={{0,2},{2,4},{4,6},{6,0},{8,10},{10,12},{12,14},{14,8},{16,18},{18,... | collective-permute-start | bytes 393224 | tf_op jit(solution)/shard_map/ppermute | solution.py:433
  54.9 24.7 %collective-permute-start.7 = (bf16[2,256,128]{2,1,0:T(8,128)(2,1)}, bf16[2,256,128]{2,1,0:T(8,128)(2,1)S(1)}, u32[]{:S(2)}, u32[]{:S(2)}) collective-permute-start(bf16[2,256,128]{2,1,0:T(8,128)(2,1)} %get-tuple-element.23), channel_id=1, source_target_pairs={{0,4},{2,6},{4,0},{6,2},{8,12},{10,14},{12,8},{14,10},{16,20},{18,... | collective-permute-start | bytes 393224 | tf_op jit(solution)/shard_map/ppermute | solution.py:433
  57.5 22.1 %collective-permute-start.8 = (bf16[2,256,128]{2,1,0:T(8,128)(2,1)}, bf16[2,256,128]{2,1,0:T(8,128)(2,1)}, u32[]{:S(2)}, u32[]{:S(2)}) collective-permute-start(bf16[2,256,128]{2,1,0:T(8,128)(2,1)} %get-tuple-element.24), channel_id=1, source_target_pairs={{0,6},{2,0},{4,2},{6,4},{8,14},{10,8},{12,10},{14,12},{16,22},{18,... | collective-permute-start | bytes 393224 | tf_op jit(solution)/shard_map/ppermute | solution.py:433
  57.5 1.0 copy-start.2
  58.5 21.1 %collective-permute-start.9 = (bf16[2,2,2,256,128]{4,3,2,1,0:T(8,128)(2,1)S(1)}, bf16[2,2,2,256,128]{4,3,2,1,0:T(8,128)(2,1)}, u32[]{:S(2)}, u32[]{:S(2)}) collective-permute-start(bf16[2,2,2,256,128]{4,3,2,1,0:T(8,128)(2,1)S(1)} %pick_last.1), channel_id=1, source_target_pairs={{0,8},{2,10},{4,12},{6,14},{8,16},{10,18},{12,20},{14,22},{16,24},... | collective-permute-start | bytes 1572872 | tf_op jit(solution)/shard_map/ppermute | solution.py:436
  65.3 26.8 %collective-permute-start.1 = (bf16[2,128,1024]{2,1,0:T(8,128)(2,1)}, bf16[2,128,1024]{2,1,0:T(8,128)(2,1)}, u32[]{:S(2)}, u32[]{:S(2)}) collective-permute-start(bf16[2,128,1024]{2,1,0:T(8,128)(2,1)} %broadcast_select_fusion), channel_id=1, source_target_pairs={{0,2},{2,4},{4,6},{6,0},{8,10},{10,12},{12,14},{14,8},{16,18},{18,... | collective-permute-start | bytes 1572872 | tf_op jit(solution)/shard_map/ppermute | solution.py:433
  65.3 14.3 %copy-start.3 = (bf16[2,2,256,128]{3,2,1,0:T(8,128)(2,1)S(1)}, bf16[2,2,256,128]{3,2,1,0:T(8,128)(2,1)}, u32[]{:S(2)}) copy-start(bf16[2,2,256,128]{3,2,1,0:T(8,128)(2,1)} %get-tuple-element.17.own_ref.refs_0_) | copy-start | bytes 786436
  65.3 14.3 %copy-start.4 = (bf16[2,256,128]{2,1,0:T(8,128)(2,1)S(1)}, bf16[2,256,128]{2,1,0:T(8,128)(2,1)}, u32[]{:S(2)}) copy-start(bf16[2,256,128]{2,1,0:T(8,128)(2,1)} %get-tuple-element.21.refs_4_) | copy-start | bytes 393220
  68.9 27.4 %all-to-all-start.1 = ((bf16[16,144,128]{2,1,0:T(8,128)(2,1)}), bf16[16,144,128]{2,1,0:T(8,128)(2,1)S(1)}, u32[]{:S(2)}, u32[]{:S(2)}) async-start(bf16[16,144,128]{2,1,0:T(8,128)(2,1)} %plane_attention.1), calls=%async_computation.1 | async-start | bytes 1179648 | tf_op jit(solution)/shard_map/all_to_all | solution.py:463
  83.0 13.3 %collective-permute-start.10 = (bf16[2,272,128]{2,1,0:T(8,128)(2,1)S(1)}, bf16[2,272,128]{2,1,0:T(8,128)(2,1)S(1)}, u32[]{:S(2)}, u32[]{:S(2)}) collective-permute-start(bf16[2,272,128]{2,1,0:T(8,128)(2,1)S(1)} %get-tuple-element.26), channel_id=1, source_target_pairs={{0,2},{2,4},{4,6},{6,0},{8,10},{10,12},{12,14},{14,8},{16,18},{18,... | collective-permute-start | bytes 417800 | tf_op jit(solution)/shard_map/ppermute | solution.py:433
  84.4 11.9 %collective-permute-start.11 = (bf16[2,272,128]{2,1,0:T(8,128)(2,1)S(1)}, bf16[2,272,128]{2,1,0:T(8,128)(2,1)S(1)}, u32[]{:S(2)}, u32[]{:S(2)}) collective-permute-start(bf16[2,272,128]{2,1,0:T(8,128)(2,1)S(1)} %get-tuple-element.27), channel_id=1, source_target_pairs={{0,4},{2,6},{4,0},{6,2},{8,12},{10,14},{12,8},{14,10},{16,20},{18,... | collective-permute-start | bytes 417800 | tf_op jit(solution)/shard_map/ppermute | solution.py:433
  86.9 9.5 %collective-permute-start.12 = (bf16[2,272,128]{2,1,0:T(8,128)(2,1)S(1)}, bf16[2,272,128]{2,1,0:T(8,128)(2,1)S(1)}, u32[]{:S(2)}, u32[]{:S(2)}) collective-permute-start(bf16[2,272,128]{2,1,0:T(8,128)(2,1)S(1)} %get-tuple-element.28), channel_id=1, source_target_pairs={{0,6},{2,0},{4,2},{6,4},{8,14},{10,8},{12,10},{14,12},{16,22},{18,... | collective-permute-start | bytes 417800 | tf_op jit(solution)/shard_map/ppermute | solution.py:433
  92.1 4.3 %copy-start = (bf16[128,1280]{1,0:T(8,128)(2,1)S(1)}, bf16[128,1280]{1,0:T(8,128)(2,1)}, u32[]{:S(2)}) copy-start(bf16[128,1280]{1,0:T(8,128)(2,1)} %near_attention.2.early_ref) | copy-start | bytes 983044
  96.4 1.0 copy-start.1
  99.2 13.6 %collective-permute-start.13 = (bf16[256,1024]{1,0:T(8,128)(2,1)S(1)}, bf16[256,1024]{1,0:T(8,128)(2,1)S(1)}, u32[]{:S(2)}, u32[]{:S(2)}) collective-permute-start(bf16[256,1024]{1,0:T(8,128)(2,1)S(1)} %merge_groups.1.in_ref), channel_id=1, source_target_pairs={{0,1},{1,0},{2,3},{3,2},{4,5},{5,4},{6,7},{7,6},{8,9},{9,8},{10,11... | collective-permute-start | bytes 1572872 | tf_op jit(solution)/shard_map/ppermute | solution.py:467
